TPU v7x, 256 devices: a whole 4x4x8 slice. The times are simulated.
256 devices in a mesh: ep: 16 (over y, x), tp: 16 (over z, core).
Axes of the slice: x: 4, y: 4, z: 8, core: 2. Of those that a mesh axis runs over, the one named last changes fastest.
Arguments:
- tokens: bfloat16 [256, 2048], P('ep'), may hold values from -6 to 6
- norm_gain: float32 [2048], replicated, may hold values from 0.1 to 1.9
- w_query: bfloat16 [2048, 2048], P('ep', 'tp'), may hold values from -0.125 to 0.125
- w_key: bfloat16 [2048, 2048], P('ep', 'tp'), may hold values from -0.125 to 0.125
- w_value: bfloat16 [2048, 2048], P('ep', 'tp'), may hold values from -0.125 to 0.125
- w_forget: bfloat16 [2048, 16], replicated, may hold values from -0.125 to 0.125
- forget_bias: float32 [16], replicated, may hold values from -1 to 2
- query_gain: float32 [128], replicated, may hold values from 0.1 to 1.9
- key_gain: float32 [128], replicated, may hold values from 0.1 to 1.9
- cache_keys: bfloat16 [256, 16, 1024, 128], P('ep', 'tp'), may hold values from -400 to 400
- cache_values: bfloat16 [256, 16, 1024, 128], P('ep', 'tp'), may hold values from -6 to 6
- cache_gates: float32 [256, 16, 1024], P('ep', 'tp'), may hold values from -144 to 0, as said below
- lengths: int32 [256], P('ep'), may hold values from 1 to 1024, 131072 in all
- w_output: bfloat16 [2048, 2048], P('tp'), may hold values from -0.375 to 0.375
- ffn_gain: float32 [2048], replicated, may hold values from 0.1 to 1.9
- routes: int32 [256, 2], P('ep'), may hold values from 0 to 31, all different within a row; in each aligned block of 16 rows (0 to 15, 16 to 31, ...) at most 2 rows name the same one
- route_weights: float32 [256, 2], P('ep'), may hold values from 0.2 to 1
- w_gate: bfloat16 [32, 2048, 2048], P('ep', None, 'tp'), may hold values from -0.125 to 0.125
- w_up: bfloat16 [32, 2048, 2048], P('ep', None, 'tp'), may hold values from -0.125 to 0.125
- w_down: bfloat16 [32, 2048, 2048], P('ep', 'tp'), may hold values from -0.125 to 0.125
Outputs:
- result: bfloat16 [256, 2048], P('ep', 'tp')
Inputs may be any that keep to these rules, and one draw needn't show every extreme that they name: `routes`: within the rows of one index of ep (16 sequences) no expert is named by more than 2 rows, a bound that some block reaches; each row names 2 different experts. `lengths`: one sequence has exactly 1024 cached positions. `cache_gates`: along positions, the values of each sequence and head never rise.
All inputs are finite; a program needn't handle non-finite values. No bound on the sum of `lengths` on one device may be relied on, other than what follows from the above.
Results may differ from a plain program's by a relative error of at most 0.012.
The roundings to bfloat16 on the way count: a program that leaves them out, or rounds other values in their place, can miss the bound.
Values may be sent and summed in bfloat16 or wider, within the bound.
A program may use at most 64 MiB of HBM per device.

v0:
```python
import jax
import jax.numpy as jnp
from jax import lax
from jax.sharding import PartitionSpec as P

epsilon = 1e-06


def cut_along(array, dim, length):
    before, after = (array.shape[:dim], array.shape[dim + 1 :])
    return jnp.moveaxis(array.reshape(*before, length, -1, *after), dim, 0)


def sum_at_owner(array, axis, dim):
    length = lax.axis_size(axis)
    parts = lax.all_to_all(cut_along(array, dim, length), axis, 0, 0, tiled=True)
    return jnp.sum(parts, axis=0)


def sent_to_all(array, axis):
    length = lax.axis_size(axis)
    return lax.all_to_all(
        jnp.broadcast_to(array[None], (length, *array.shape)), axis, 0, 0, tiled=True
    )


def of_everyone(array, axis):
    everything = sent_to_all(array, axis)
    return jnp.sum(everything, axis=0)


def sum_at_owner_2(array, axis, dim):
    parts = cut_along(array, dim, lax.axis_size(axis))
    arrived = lax.all_to_all(parts, axis, split_axis=0, concat_axis=0, tiled=True)
    return arrived.astype(jnp.float32).sum(axis=0)


def norm_rows(values, gain_row):
    widened = values.astype(jnp.float32)
    scaled = widened * lax.rsqrt(jnp.mean(widened * widened, axis=-1, keepdims=True) + epsilon)
    return scaled * gain_row


def local(
    tokens,
    norm_gain,
    w_query,
    w_key,
    w_value,
    w_forget,
    forget_bias,
    query_gain,
    key_gain,
    cache_keys,
    cache_values,
    cache_gates,
    lengths,
    w_output,
    ffn_gain,
    routes,
    route_weights,
    w_gate,
    w_up,
    w_down,
):
    group_rows = tokens.shape[0]
    model_width = tokens.shape[1]
    heads_local = cache_keys.shape[1]
    cache_span = cache_keys.shape[2]
    head_size = cache_keys.shape[3]
    local_cols = w_query.shape[1]
    normed = norm_rows(tokens, norm_gain).astype(jnp.bfloat16)
    blocks = lax.all_to_all(normed, "ep", split_axis=1, concat_axis=0, tiled=True)
    summed = sum_at_owner(
        jnp.concatenate(
            [
                jnp.dot(blocks, w_query, preferred_element_type=jnp.float32),
                jnp.dot(blocks, w_key, preferred_element_type=jnp.float32),
                jnp.dot(blocks, w_value, preferred_element_type=jnp.float32),
            ],
            axis=1,
        ),
        "ep",
        0,
    )
    query_raw = summed[:, :local_cols]
    key_raw = summed[:, local_cols : 2 * local_cols]
    value_raw = summed[:, 2 * local_cols :]
    queries = norm_rows(query_raw.reshape(group_rows, heads_local, head_size), query_gain).astype(
        jnp.bfloat16
    )
    keys_new = norm_rows(key_raw.reshape(group_rows, heads_local, head_size), key_gain).astype(
        jnp.bfloat16
    )
    values_new = value_raw.reshape(group_rows, heads_local, head_size).astype(jnp.bfloat16)
    biased = jnp.dot(normed, w_forget, preferred_element_type=jnp.float32) + forget_bias
    forget = jax.nn.log_sigmoid(
        lax.dynamic_slice_in_dim(biased, lax.axis_index("tp") * heads_local, heads_local, 1)
    )
    score_scale = head_size ** (-0.5)
    positions = jnp.arange(cache_span, dtype=jnp.int32)
    live_mask = positions[None, :] < lengths[:, None]
    ending = positions[None, :] == lengths[:, None] - 1
    last_gate = jnp.sum(jnp.where(ending[:, None, :], cache_gates, 0.0), axis=-1)
    scores = (
        jnp.einsum("bhd,bhld->bhl", queries, cache_keys, preferred_element_type=jnp.float32)
        * score_scale
    )
    scores = scores + (last_gate[:, :, None] - cache_gates) + forget[:, :, None]
    scores = jnp.where(live_mask[:, None, :], scores, -1e30)
    own_score = (
        jnp.sum(queries.astype(jnp.float32) * keys_new.astype(jnp.float32), axis=-1) * score_scale
    )
    row_peak = jnp.maximum(jnp.max(scores, axis=-1), own_score)
    weights = jnp.exp(scores - row_peak[:, :, None])
    own_weight = jnp.exp(own_score - row_peak)
    denominator = jnp.sum(weights, axis=-1) + own_weight
    probabilities = (weights / denominator[:, :, None]).astype(jnp.bfloat16)
    own_prob = (own_weight / denominator).astype(jnp.bfloat16)
    attended = jnp.einsum(
        "bhl,bhld->bhd", probabilities, cache_values, preferred_element_type=jnp.float32
    )
    attended = attended + own_prob.astype(jnp.float32)[:, :, None] * values_new.astype(jnp.float32)
    attended = attended.astype(jnp.bfloat16).reshape(group_rows, heads_local * head_size)
    partial_value = jnp.dot(attended, w_output, preferred_element_type=jnp.float32)
    slice_width = model_width // lax.axis_size("tp")
    col_start = lax.axis_index("tp") * slice_width
    own_tokens = lax.dynamic_slice_in_dim(tokens, col_start, slice_width, 1)
    share_sum = sum_at_owner(partial_value, "tp", 1)
    mixed_cols = (own_tokens.astype(jnp.float32) + share_sum).astype(jnp.bfloat16)
    widened = mixed_cols.astype(jnp.float32)
    square_total = of_everyone(jnp.sum(widened * widened, axis=1), "tp")
    gain_cols = lax.dynamic_slice_in_dim(ffn_gain, col_start, slice_width, 0)
    scaled = widened * lax.rsqrt(square_total / model_width + epsilon)[:, None]
    dispatch_rows = (scaled * gain_cols[None, :]).astype(jnp.bfloat16)
    experts_local = w_gate.shape[0]
    ep_count = lax.axis_size("ep")
    expert_total = experts_local * ep_count
    top_count = routes.shape[1]
    capacity = 2 * group_rows * top_count // expert_total
    slot_total = expert_total * capacity
    item_total = group_rows * top_count
    flat_routes = routes.reshape(item_total)
    matches = (flat_routes[:, None] == jnp.arange(expert_total, dtype=jnp.int32)[None, :]).astype(
        jnp.int32
    )
    earlier = jnp.cumsum(matches, axis=0) - matches
    slot_index = flat_routes * capacity + jnp.sum(earlier * matches, axis=1)
    slot_match = (jnp.arange(slot_total, dtype=jnp.int32)[:, None] == slot_index[None, :]).astype(
        jnp.float32
    )
    item_owner = (
        (jnp.arange(item_total, dtype=jnp.int32) // top_count)[:, None]
        == jnp.arange(group_rows, dtype=jnp.int32)[None, :]
    ).astype(jnp.float32)
    placing = jnp.dot(slot_match, item_owner, precision=lax.Precision.HIGHEST)
    outgoing = jnp.dot(
        placing.astype(jnp.bfloat16), dispatch_rows, preferred_element_type=jnp.float32
    )
    outgoing = outgoing.astype(jnp.bfloat16).reshape(
        ep_count, experts_local, capacity, dispatch_rows.shape[1]
    )
    arrived = lax.all_to_all(outgoing, "ep", split_axis=0, concat_axis=0, tiled=True)
    arrived = lax.all_gather(arrived, "tp", axis=3, tiled=True)
    gate_part = jnp.einsum("sxcd,xdf->sxcf", arrived, w_gate, preferred_element_type=jnp.float32)
    upper_part = jnp.einsum("sxcd,xdf->sxcf", arrived, w_up, preferred_element_type=jnp.float32)
    hidden = (jax.nn.silu(gate_part) * upper_part).astype(jnp.bfloat16)
    partial_out = jnp.einsum("sxcf,xfd->sxcd", hidden, w_down, preferred_element_type=jnp.float32)
    shares = sum_at_owner_2(partial_out.astype(jnp.bfloat16), "tp", 3)
    returned = lax.all_to_all(
        shares.astype(jnp.bfloat16), "ep", split_axis=0, concat_axis=0, tiled=True
    )
    flat_returned = returned.reshape(slot_total, slice_width)
    fractions = route_weights / jnp.sum(route_weights, axis=-1, keepdims=True)
    slot_grid = slot_index.reshape(group_rows, top_count)
    combine = jnp.sum(
        jnp.where(
            slot_grid[:, :, None] == jnp.arange(slot_total, dtype=jnp.int32)[None, None, :],
            fractions[:, :, None],
            0.0,
        ),
        axis=1,
    )
    expert_mix = jnp.dot(
        combine, flat_returned.astype(jnp.float32), precision=lax.Precision.HIGHEST
    )
    return (mixed_cols.astype(jnp.float32) + expert_mix).astype(jnp.bfloat16)


def solution(mesh):
    placed = (
        P("ep", None),
        P(),
        P("ep", "tp"),
        P("ep", "tp"),
        P("ep", "tp"),
        P(),
        P(),
        P(),
        P(),
        P("ep", "tp", None, None),
        P("ep", "tp", None, None),
        P("ep", "tp", None),
        P("ep"),
        P("tp", None),
        P(),
        P("ep", None),
        P("ep", None),
        P("ep", None, "tp"),
        P("ep", None, "tp"),
        P("ep", "tp", None),
    )
    return jax.shard_map(
        local, mesh=mesh, in_specs=placed, out_specs=P("ep", "tp"), check_vma=False
    )
```

profile of v0, /device:TPU:1, one launch (start us, length us, event | category | flops | bytes accessed | tf_op | source)
XLA Modules:
  0.0 127.4 jit_solution(13908288329338622491)
XLA Ops:
  0.0 1.1 fusion.12
  1.1 1.6 %copy_bitcast_fusion = bf16[16,16,128]{2,0,1:T(8,128)(2,1)} fusion(f32[2048]{0:T(1024)} %param.21, f32[16]{0:T(128)S(1)} %add_rsqrt_fusion.3, bf16[16,2048]{1,0:T(8,128)(2,1)} %param.20), kind=kLoop, calls=%fused_computation.27 | loop fusion | flops 131072 | bytes 139328 | tf_op jit(solution)/shard_map/all_to_all | solution.py:73
  2.7 7.6 %all-to-all-start = ((bf16[16,16,128]{2,0,1:T(8,128)(2,1)}), bf16[16,16,128]{2,0,1:T(8,128)(2,1)S(1)}, u32[]{:S(2)}, u32[]{:S(2)}) async-start(bf16[16,16,128]{2,0,1:T(8,128)(2,1)} %copy_bitcast_fusion), calls=%async_computation | async-start | bytes 131072 | tf_op jit(solution)/shard_map/all_to_all | solution.py:73
  10.2 1.1 fusion.28
  11.3 0.8 copy.100
  12.3 1.2 dynamic-slice
  13.5 3.2 %all-to-all-done = bf16[16,16,128]{2,0,1:T(8,128)(2,1)S(1)} async-done(((bf16[16,16,128]{2,0,1:T(8,128)(2,1)}), bf16[16,16,128]{2,0,1:T(8,128)(2,1)S(1)}, u32[]{:S(2)}, u32[]{:S(2)}) %all-to-all-start) | async-done | bytes 65568 | tf_op jit(solution)/shard_map/all_to_all | solution.py:73
  16.8 1.0 fusion.50
  17.7 1.0 fusion.51
  18.7 1.0 fusion.52
  19.7 0.9 copy.98
  20.6 3.6 %all-to-all-start.1 = ((f32[16,16,384]{2,1,0:T(8,128)}), f32[16,16,384]{2,1,0:T(8,128)S(1)}, u32[]{:S(2)}, u32[]{:S(2)}) async-start(f32[16,16,384]{2,1,0:T(8,128)} %bitcast.3), calls=%async_computation.1 | async-start | bytes 786432 | tf_op jit(solution)/shard_map/all_to_all | solution.py:16
  24.9 1.3 %copy.114 = bf16[2048,128]{1,0:T(8,128)(2,1)S(1)} copy(bf16[2048,128]{0,1:T(8,128)(2,1)} %bitcast.88) | data formatting | bytes 1048576 | tf_op jit(solution)/shard_map/dot_general | solution.py:125
  26.6 6.1 %all-to-all-done.1 = f32[16,16,384]{2,1,0:T(8,128)S(1)} async-done(((f32[16,16,384]{2,1,0:T(8,128)}), f32[16,16,384]{2,1,0:T(8,128)S(1)}, u32[]{:S(2)}, u32[]{:S(2)}) %all-to-all-start.1) | async-done | bytes 393248 | tf_op jit(solution)/shard_map/all_to_all | solution.py:16
  33.0 3.5 %fusion.2 = f32[16,1,1024]{2,1,0:T(1,128)S(1)} fusion(bf16[16,1,1024,128]{3,2,1,0:T(8,128)(2,1)} %param.29, bf16[16,128,1]{1,0,2:T(8,128)(2,1)S(1)} %get-tuple-element.12), kind=kOutput, calls=%fused_computation.2 | convolution fusion | flops 4194304 | bytes 4263936 | tf_op jit(solution)/shard_map/bhd,bhld->bhl/dot_general | solution.py:106
  37.3 0.7 fusion
  38.0 0.9 convolution_bitcast_fusion
  39.0 11.5 %all-to-all-start.2 = ((f32[16,16,128]{2,1,0:T(8,128)}), f32[16,16,128]{2,1,0:T(8,128)S(1)}, u32[]{:S(2)}, u32[]{:S(2)}) async-start(f32[16,16,128]{2,1,0:T(8,128)} %convolution_bitcast_fusion), calls=%async_computation.2 | async-start | bytes 262144 | tf_op jit(solution)/shard_map/all_to_all | solution.py:16
  50.6 8.7 %all-to-all-done.2 = f32[16,16,128]{2,1,0:T(8,128)S(1)} async-done(((f32[16,16,128]{2,1,0:T(8,128)}), f32[16,16,128]{2,1,0:T(8,128)S(1)}, u32[]{:S(2)}, u32[]{:S(2)}) %all-to-all-start.2) | async-done | bytes 131104 | tf_op jit(solution)/shard_map/all_to_all | solution.py:16
  59.4 0.8 fusion.31
  60.8 3.3 %all-to-all-start.3 = ((f32[16,1,16]{2,1,0:T(1,128)}), f32[16,1,16]{2,1,0:T(1,128)S(1)}, u32[]{:S(2)}, u32[]{:S(2)}) async-start(f32[16,1,16]{2,1,0:T(1,128)} %broadcast_in_dim.21), calls=%async_computation.3 | async-start | bytes 16384 | tf_op jit(solution)/shard_map/all_to_all | solution.py:22
  64.3 0.8 dynamic_slice.11
  65.1 5.9 %all-to-all-done.3 = f32[16,1,16]{2,1,0:T(1,128)S(1)} async-done(((f32[16,1,16]{2,1,0:T(1,128)}), f32[16,1,16]{2,1,0:T(1,128)S(1)}, u32[]{:S(2)}, u32[]{:S(2)}) %all-to-all-start.3) | async-done | bytes 1056 | tf_op jit(solution)/shard_map/all_to_all | solution.py:22
  71.2 9.1 %all_to_all.50 = bf16[16,2,2,128]{3,2,1,0:T(2,128)(2,1)S(1)} all-to-all(bf16[16,2,2,128]{3,2,1,0:T(2,128)(2,1)S(1)} %bitcast.91), channel_id=1, replica_groups=mesh['ep'=16,'tp'=16] {'ep'}, dimensions={0} | all-to-all | bytes 32768 | tf_op jit(solution)/shard_map/all_to_all | solution.py:163
  80.3 17.3 %all_gather.3 = bf16[16,2,2,2048]{3,0,2,1:T(8,128)(2,1)S(1)} all-gather(bf16[16,2,2,128]{3,0,2,1:T(8,128)(2,1)S(1)} %copy.103), channel_id=1, replica_groups=mesh['ep'=16,'tp'=16] {'tp'}, dimensions={3}, use_global_device_ids=true | all-gather | bytes 278528 | tf_op jit(solution)/shard_map/all_gather | solution.py:164
  97.9 1.7 %fusion.4 = bf16[2,2,2,16,8,128]{5,4,3,2,1,0:T(8,128)(2,1)S(1)} fusion(bf16[2,128,2048]{2,1,0:T(8,128)(2,1)S(1)} %copy-done, bf16[16,2,2,2048]{3,0,2,1:T(8,128)(2,1)S(1)} %all_gather.3, bf16[2,2048,128]{2,1,0:T(8,128)(2,1)} %param.38, f32[16,2,2,128]{3,0,2,1:T(8,128)S(1)} %convolution_bitcast_fusion.2), kind=kOutput, calls=%fused_computation.5 | convolution fusion | flops 67289088 | bytes 2654208 | tf_op jit(solution)/shard_map/sxcf,xfd->sxcd/dot_general | solution.py:168
  99.6 0.8 copy.123
  100.3 4.1 %all-to-all-start.5 = ((bf16[16,16,2,2,128]{4,1,3,2,0:T(8,128)(2,1)}), bf16[16,16,2,2,128]{4,1,3,2,0:T(8,128)(2,1)S(1)}, u32[]{:S(2)}, u32[]{:S(2)}) async-start(bf16[16,16,2,2,128]{4,1,3,2,0:T(8,128)(2,1)} %bitcast.83), calls=%async_computation.5 | async-start | bytes 524288 | tf_op jit(solution)/shard_map/all_to_all | solution.py:34
  104.7 11.4 %all-to-all-done.5 = bf16[16,16,2,2,128]{4,1,3,2,0:T(8,128)(2,1)S(1)} async-done(((bf16[16,16,2,2,128]{4,1,3,2,0:T(8,128)(2,1)}), bf16[16,16,2,2,128]{4,1,3,2,0:T(8,128)(2,1)S(1)}, u32[]{:S(2)}, u32[]{:S(2)}) %all-to-all-start.5) | async-done | bytes 262176 | tf_op jit(solution)/shard_map/all_to_all | solution.py:34
  116.7 3.5 %all-to-all-start.6 = ((bf16[16,2,2,128]{3,2,1,0:T(2,128)(2,1)}), bf16[16,2,2,128]{3,2,1,0:T(2,128)(2,1)S(1)}, u32[]{:S(2)}, u32[]{:S(2)}) async-start(bf16[16,2,2,128]{3,2,1,0:T(2,128)(2,1)} %copy.106), calls=%async_computation.6 | async-start | bytes 32768 | tf_op jit(solution)/shard_map/all_to_all | solution.py:170
  120.3 6.4 %all-to-all-done.6 = bf16[16,2,2,128]{3,2,1,0:T(2,128)(2,1)S(1)} async-done(((bf16[16,2,2,128]{3,2,1,0:T(2,128)(2,1)}), bf16[16,2,2,128]{3,2,1,0:T(2,128)(2,1)S(1)}, u32[]{:S(2)}, u32[]{:S(2)}) %all-to-all-start.6) | async-done | bytes 16416 | tf_op jit(solution)/shard_map/all_to_all | solution.py:170
  126.7 0.7 fusion.7
  (53 shorter events, 4.8 us)
Async XLA Ops:
  0.0 97.9 %copy-start = (bf16[2,128,2048]{2,1,0:T(8,128)(2,1)S(1)}, bf16[2,128,2048]{2,1,0:T(8,128)(2,1)}, u32[]{:S(2)}) copy-start(bf16[2,128,2048]{2,1,0:T(8,128)(2,1)} %param.39) | copy-start | bytes 3145732
  0.0 26.2 %copy-start.5 = (s32[16]{0:T(128)S(1)}, s32[16]{0:T(128)}, u32[]{:S(2)}) copy-start(s32[16]{0:T(128)} %param.32) | copy-start | bytes 196
  0.0 26.2 %copy-start.2 = (f32[16,1,1024]{2,1,0:T(1,128)S(1)}, f32[16,1,1024]{2,1,0:T(1,128)}, u32[]{:S(2)}) copy-start(f32[16,1,1024]{2,1,0:T(1,128)} %param.31) | copy-start | bytes 196612
  0.0 32.8 %copy-start.7 = (f32[128]{0:T(128)S(1)}, f32[128]{0:T(128)}, u32[]{:S(2)}) copy-start(f32[128]{0:T(128)} %param.27) | copy-start | bytes 1540
  0.0 32.8 %copy-start.6 = (f32[128]{0:T(128)S(1)}, f32[128]{0:T(128)}, u32[]{:S(2)}) copy-start(f32[128]{0:T(128)} %param.28) | copy-start | bytes 1540
  2.7 14.1 %all-to-all-start = ((bf16[16,16,128]{2,0,1:T(8,128)(2,1)}), bf16[16,16,128]{2,0,1:T(8,128)(2,1)S(1)}, u32[]{:S(2)}, u32[]{:S(2)}) async-start(bf16[16,16,128]{2,0,1:T(8,128)(2,1)} %copy_bitcast_fusion), calls=%async_computation | async-start | bytes 131072 | tf_op jit(solution)/shard_map/all_to_all | solution.py:73
  20.6 12.0 %all-to-all-start.1 = ((f32[16,16,384]{2,1,0:T(8,128)}), f32[16,16,384]{2,1,0:T(8,128)S(1)}, u32[]{:S(2)}, u32[]{:S(2)}) async-start(f32[16,16,384]{2,1,0:T(8,128)} %bitcast.3), calls=%async_computation.1 | async-start | bytes 786432 | tf_op jit(solution)/shard_map/all_to_all | solution.py:16
  32.7 4.6 %copy-start.8 = (bf16[16,1,1024,128]{3,2,1,0:T(8,128)(2,1)S(1)}, bf16[16,1,1024,128]{3,2,1,0:T(8,128)(2,1)}, u32[]{:S(2)}) copy-start(bf16[16,1,1024,128]{3,2,1,0:T(8,128)(2,1)} %param.30) | copy-start | bytes 12582916
  36.6 61.0 %copy-start.1 = (bf16[2,2048,128]{2,1,0:T(8,128)(2,1)S(1)}, bf16[2,2048,128]{2,1,0:T(8,128)(2,1)}, u32[]{:S(2)}) copy-start(bf16[2,2048,128]{2,1,0:T(8,128)(2,1)} %param.37) | copy-start | bytes 3145732
  38.0 66.6 %copy-start.4 = (f32[16,2]{0,1:T(2,128)S(1)}, f32[16,2]{0,1:T(2,128)}, u32[]{:S(2)}) copy-start(f32[16,2]{0,1:T(2,128)} %param.36) | copy-start | bytes 388
  38.0 66.7 %copy-start.3 = (s32[16,2]{0,1:T(2,128)S(1)}, s32[16,2]{0,1:T(2,128)}, u32[]{:S(2)}) copy-start(s32[16,2]{0,1:T(2,128)} %param.35) | copy-start | bytes 388
  39.0 20.4 %all-to-all-start.2 = ((f32[16,16,128]{2,1,0:T(8,128)}), f32[16,16,128]{2,1,0:T(8,128)S(1)}, u32[]{:S(2)}, u32[]{:S(2)}) async-start(f32[16,16,128]{2,1,0:T(8,128)} %convolution_bitcast_fusion), calls=%async_computation.2 | async-start | bytes 262144 | tf_op jit(solution)/shard_map/all_to_all | solution.py:16
  60.8 10.2 %all-to-all-start.3 = ((f32[16,1,16]{2,1,0:T(1,128)}), f32[16,1,16]{2,1,0:T(1,128)S(1)}, u32[]{:S(2)}, u32[]{:S(2)}) async-start(f32[16,1,16]{2,1,0:T(1,128)} %broadcast_in_dim.21), calls=%async_computation.3 | async-start | bytes 16384 | tf_op jit(solution)/shard_map/all_to_all | solution.py:22
  100.3 15.7 %all-to-all-start.5 = ((bf16[16,16,2,2,128]{4,1,3,2,0:T(8,128)(2,1)}), bf16[16,16,2,2,128]{4,1,3,2,0:T(8,128)(2,1)S(1)}, u32[]{:S(2)}, u32[]{:S(2)}) async-start(bf16[16,16,2,2,128]{4,1,3,2,0:T(8,128)(2,1)} %bitcast.83), calls=%async_computation.5 | async-start | bytes 524288 | tf_op jit(solution)/shard_map/all_to_all | solution.py:34
  116.7 10.0 %all-to-all-start.6 = ((bf16[16,2,2,128]{3,2,1,0:T(2,128)(2,1)}), bf16[16,2,2,128]{3,2,1,0:T(2,128)(2,1)S(1)}, u32[]{:S(2)}, u32[]{:S(2)}) async-start(bf16[16,2,2,128]{3,2,1,0:T(2,128)(2,1)} %copy.106), calls=%async_computation.6 | async-start | bytes 32768 | tf_op jit(solution)/shard_map/all_to_all | solution.py:170
where the time goes:
time: 128 us; the launch traced here: 127 us
  waiting for transfers between devices  41.7 us (33%)
  starting transfers between devices  33.5 us (26%)
  blocking collectives  26.3 us (21%)
  matrix products  12.3 us (10%)
  local copies, waits for them, and re-layouts  7.28 us (6%)
  other arithmetic  6.01 us (5%)
    all_gather x1, blocking collectives, local(): arrived = lax.all_gather(arrived, 'tp', axis=3, tiled=True)  17.3 us
    all_to_all x2, starting transfers between devices, sum_at_owner(): lax.all_to_all(cut_along(array, dim, length), axis, 0, 0, tiled=True)  15 us
    all_to_all x2, waiting for transfers between devices, sum_at_owner(): lax.all_to_all(cut_along(array, dim, length), axis, 0, 0, tiled=True)  14.8 us
    all_to_all x1, waiting for transfers between devices, sum_at_owner_2(): lax.all_to_all(parts, axis, split_axis=0, concat_axis=0, tiled=True)  11.4 us
    all_to_all x1, blocking collectives, local(): lax.all_to_all(outgoing, 'ep', split_axis=0, concat_axis=0, tiled=True)  9.05 us
    all_to_all x1, starting transfers between devices, local(): lax.all_to_all(normed, 'ep', split_axis=1, concat_axis=0, tiled=True)  7.57 us
    all_to_all x1, waiting for transfers between devices, local(): lax.all_to_all(shares.astype(jnp.bfloat16), 'ep', split_axis=0, concat_ax...  6.41 us
    all_to_all x1, waiting for transfers between devices, sent_to_all(): lax.all_to_all(jnp.broadcast_to(array[None], (length, *array.shape)), axi...  5.92 us
  transfers between devices with their start and end apart: 6, of which 6 were waited for; matrix products, arithmetic and copies ran while one was open for 6% of the time, Pallas kernels for 0%

commit v1 on v0

v1 whole, which is shorter than its diff:
```python
import functools

import jax
import jax.numpy as jnp
from jax import lax
from jax.experimental import pallas as pl
from jax.experimental.pallas import tpu as pltpu
from jax.sharding import PartitionSpec as P

MESH = pl.DeviceIdType.MESH
F32 = jnp.float32
BF16 = jnp.bfloat16
EPS = 1e-06
CAP = 2
LANES = 128

CH_X, CH_Q, CH_KV, CH_O, CH_M, CH_D, CH_R, CH_F = range(8)


def norm(v, gain):
    return v * lax.rsqrt(jnp.mean(v * v, axis=-1, keepdims=True) + EPS) * gain


def dot(a, b):
    return jnp.dot(a, b, preferred_element_type=F32)


def dot_t(a, b):
    return lax.dot_general(a, b, (((1,), (1,)), ((), ())), preferred_element_type=F32)


def swap_halves(a, b):
    low = lax.broadcasted_iota(jnp.int32, a.shape, 1) < 4
    a_turned, b_turned = pltpu.roll(a, 4, 1), pltpu.roll(b, 4, 1)
    return jnp.where(low, a, b_turned), jnp.where(low, a_turned, b)


def kernel(ep, tp, *refs):
    names = (
        "tokens", "norm_gain", "wq", "wk", "wv", "wf", "f_bias", "q_gain", "k_gain", "keys",
        "values", "gates", "lengths", "wo", "ffn_gain", "routes", "r_weights", "wg", "wu", "wd",
    )
    hbm = dict(zip(names, refs))
    out_ref = refs[len(names)]
    (
        tok_v, ng_v, wqkv_v, wf_v, fb_v, qg_v, kg_v, k_v, v_v, g_v, len_v,
        wo_v, fg_v, rt_v, rw_v, wgu_v, wd_v,
        xs, xr, qs, qr, kvs, kvr, os_, or_, ms, mr, ds_, dr, rs, rr, fs, fr,
        big, xe,
        hsem, ssem, rsem,
    ) = refs[len(names) + 1 :]

    me_e, me_t = lax.axis_index("ep"), lax.axis_index("tp")
    rows, width = tok_v.shape
    span, hd = k_v.shape[1], k_v.shape[2]
    n_blocks = width // LANES
    depth = xs.shape[2]
    slots = 2 * CAP
    n_slots = ep * slots

    fetches = {}

    def fetch(name, pairs):
        fetches[name] = []
        for src, dst in pairs:
            at = sum(len(f) for f in fetches.values())
            copy = pltpu.make_async_copy(src, dst, hsem.at[at])
            copy.start()
            fetches[name].append(copy)

    def need(*which):
        for name in which:
            for copy in fetches[name]:
                copy.wait()

    fetch("tok", [(hbm["tokens"], tok_v), (hbm["norm_gain"], ng_v)])
    fetch(
        "wqkv",
        [(hbm[w], wqkv_v.at[:, pl.ds(i * hd, hd)]) for i, w in enumerate(("wq", "wk", "wv"))],
    )
    fetch(
        "small",
        [
            (hbm["wf"], wf_v), (hbm["f_bias"], fb_v), (hbm["q_gain"], qg_v),
            (hbm["k_gain"], kg_v), (hbm["gates"], g_v), (hbm["lengths"], len_v),
            (hbm["ffn_gain"], fg_v), (hbm["routes"], rt_v), (hbm["r_weights"], rw_v),
        ],
    )
    quarter = rows // 4
    fetch(
        "k",
        [(hbm["keys"].at[pl.ds(i * quarter, quarter), 0], k_v.at[pl.ds(i * quarter, quarter)]) for i in range(4)],
    )
    fetch(
        "v",
        [(hbm["values"].at[pl.ds(i * quarter, quarter), 0], v_v.at[pl.ds(i * quarter, quarter)]) for i in range(4)],
    )
    fetch("wo", [(hbm["wo"], wo_v)])
    hidden = hbm["wg"].shape[2]
    fetch(
        "wgu",
        [
            (hbm[w].at[x], wgu_v.at[:, pl.ds((2 * x + i) * hidden, hidden)])
            for x in range(2)
            for i, w in enumerate(("wg", "wu"))
        ],
    )
    fetch("wd", [(hbm["wd"].at[x], wd_v.at[pl.ds(x * hidden, hidden)]) for x in range(2)])

    barrier = pltpu.get_barrier_semaphore()

    def greet(axis, me, n):
        def body(i, carry):
            pl.semaphore_signal(
                barrier, inc=1, device_id={axis: lax.rem(me + i, n)}, device_id_type=MESH
            )
            return carry

        lax.fori_loop(1, n, body, 0)

    greet("ep", me_e, ep)
    greet("tp", me_t, tp)

    def send(axis, me, n, channel, src, dst):
        def body(i, carry):
            peer = lax.rem(me + i, n)
            pltpu.make_async_remote_copy(
                src_ref=src(peer),
                dst_ref=dst.at[me],
                send_sem=ssem.at[channel],
                recv_sem=rsem.at[channel],
                device_id={axis: peer},
                device_id_type=MESH,
            ).start()
            return carry

        lax.fori_loop(1, n, body, 0)

    def wait_all(n, sem, buf):
        part = buf.at[pl.ds(0, n - 1)]
        pltpu.make_async_copy(part, part, sem).wait()

    need("tok")
    normed = norm(tok_v[...].astype(F32), ng_v[...]).astype(BF16)
    for j in range(ep):
        xs[j] = normed[:, j * depth : (j + 1) * depth]
    xr[pl.ds(me_e, 1)] = xs[pl.ds(me_e, 1)]
    pl.semaphore_wait(barrier, ep + tp - 2)
    send("ep", me_e, ep, CH_X, lambda j: xs.at[j], xr)

    need("small")
    row = lax.broadcasted_iota(jnp.int32, (rows, 1), 0)
    diagonal = lax.broadcasted_iota(jnp.int32, (rows, rows), 0) == lax.broadcasted_iota(
        jnp.int32, (rows, rows), 1
    )

    def as_column(line):
        return jnp.sum(jnp.where(diagonal, line, jnp.zeros_like(line)), axis=1, keepdims=True)

    biased = dot_t(normed, wf_v[...]) + fb_v[...]
    own_head = lax.broadcasted_iota(jnp.int32, biased.shape, 1) == me_t
    biased = jnp.sum(jnp.where(own_head, biased, 0.0), axis=1, keepdims=True)
    forget = jnp.minimum(biased, 0.0) - jnp.log1p(jnp.exp(-jnp.abs(biased)))

    lengths = as_column(len_v[...].astype(F32)).astype(jnp.int32)
    position = lax.broadcasted_iota(jnp.int32, (rows, span), 1)
    gates = jnp.zeros((rows, span), F32)
    for s in range(rows):
        gates = jnp.where(row == s, g_v[s], gates)
    last_gate = jnp.sum(jnp.where(position == lengths - 1, gates, 0.0), axis=1, keepdims=True)
    live = position < lengths

    first = rt_v[0:1, :]
    second = rt_v[1:2, :]
    slot_col = lax.broadcasted_iota(jnp.int32, (n_slots, rows), 0)
    expert_col, copy_col = lax.div(slot_col, CAP), lax.rem(slot_col, CAP)
    named = ((expert_col == first) | (expert_col == second)).astype(F32)
    before = (
        lax.broadcasted_iota(jnp.int32, (rows, rows), 0)
        < lax.broadcasted_iota(jnp.int32, (rows, rows), 1)
    ).astype(F32)
    earlier = dot(named.astype(BF16), before.astype(BF16))
    placing = jnp.where(earlier == copy_col.astype(F32), named, 0.0).astype(BF16)

    weight_sum = rw_v[0:1, :] + rw_v[1:2, :]
    share_a = as_column(rw_v[0:1, :] / weight_sum)
    share_b = as_column(rw_v[1:2, :] / weight_sum)
    route_a = as_column(first.astype(F32)).astype(jnp.int32)
    route_b = as_column(second.astype(F32)).astype(jnp.int32)
    slot_row = lax.broadcasted_iota(jnp.int32, (rows, n_slots), 1)
    expert_row, copy_row = lax.div(slot_row, CAP), lax.rem(slot_row, CAP)
    is_a, is_b = expert_row == route_a, expert_row == route_b
    after = (
        lax.broadcasted_iota(jnp.int32, (rows, rows), 1)
        < lax.broadcasted_iota(jnp.int32, (rows, rows), 0)
    ).astype(BF16)
    earlier_row = dot(after, (is_a | is_b).astype(F32).astype(BF16))
    combine = jnp.where(is_a, share_a, 0.0) + jnp.where(is_b, share_b, 0.0)
    combine = jnp.where(earlier_row == copy_row.astype(F32), combine, 0.0)
    combine_1 = combine.astype(BF16)
    rest = combine - combine_1.astype(F32)
    combine_2 = rest.astype(BF16)
    combine_3 = (rest - combine_2.astype(F32)).astype(BF16)
    combine_parts = jnp.concatenate([combine_1, combine_2, combine_3], axis=0)

    need("wqkv")
    wait_all(ep, rsem.at[CH_X], xr)
    part = dot(xr[...].reshape(ep * rows, depth), wqkv_v[...])
    qs[...] = part[:, :hd].reshape(ep, rows, hd)
    for j in range(ep):
        own = part[j * rows : (j + 1) * rows]
        kvs[j, 0:rows, :] = own[:, hd : 2 * hd].astype(BF16)
        kvs[j, rows : 2 * rows, :] = own[:, 2 * hd :].astype(BF16)
    qr[pl.ds(me_e, 1)] = qs[pl.ds(me_e, 1)]
    kvr[pl.ds(me_e, 1)] = kvs[pl.ds(me_e, 1)]
    send("ep", me_e, ep, CH_Q, lambda j: qs.at[j], qr)
    send("ep", me_e, ep, CH_KV, lambda j: kvs.at[j], kvr)
    need("k", "v")
    wait_all(ep, rsem.at[CH_Q], qr)
    queries = norm(jnp.sum(qr[...], axis=0), qg_v[...]).astype(BF16)

    score_scale = hd ** (-0.5)
    scores = jnp.zeros((rows, span), F32)
    for s in range(rows):
        scores = jnp.where(row == s, dot_t(queries, k_v[s]), scores)
    wait_all(ep, rsem.at[CH_KV], kvr)
    kv_raw = jnp.sum(kvr[...].astype(F32), axis=0)
    keys_new = norm(kv_raw[:rows], kg_v[...]).astype(BF16)
    values_new = kv_raw[rows:].astype(BF16)
    scores = scores * score_scale + (last_gate - gates) + forget
    scores = jnp.where(live, scores, -1e30)
    own_score = (
        jnp.sum(queries.astype(F32) * keys_new.astype(F32), axis=1, keepdims=True) * score_scale
    )
    peak = jnp.maximum(jnp.max(scores, axis=1, keepdims=True), own_score)
    weights = jnp.exp(scores - peak)
    own_weight = jnp.exp(own_score - peak)
    denominator = jnp.sum(weights, axis=1, keepdims=True) + own_weight
    probabilities = weights / denominator
    own_prob = (own_weight / denominator).astype(BF16).astype(F32)
    attended = own_prob * values_new.astype(F32)
    for s in range(rows):
        mine = jnp.where(row == s, probabilities, 0.0).astype(BF16)
        attended = attended + dot(mine, v_v[s])
    attended = attended.astype(BF16)

    need("wo")
    cols = or_.shape[2]
    partial = dot(attended, wo_v[...])
    for j in range(tp):
        os_[j] = partial[:, j * cols : (j + 1) * cols]
    or_[pl.ds(me_t, 1)] = os_[pl.ds(me_t, 1)]
    send("tp", me_t, tp, CH_O, lambda j: os_.at[j], or_)
    wait_all(tp, rsem.at[CH_O], or_)
    own_tokens = tok_v[:, pl.ds(pl.multiple_of(me_t * cols, cols), cols)].astype(F32)
    mixed = (own_tokens + jnp.sum(or_[...], axis=0)).astype(BF16)
    ms[...] = mixed
    mr[pl.ds(me_t, 1)] = mixed[None]
    send("tp", me_t, tp, CH_M, lambda j: ms, mr)
    need("wgu", "wd")
    wait_all(tp, rsem.at[CH_M], mr)

    squares = jnp.zeros((rows, 1), F32)
    for b in range(n_blocks):
        block = mr[b].astype(F32)
        squares = squares + jnp.sum(block * block, axis=1, keepdims=True)
    factor = lax.rsqrt(squares / width + EPS)
    for b in range(n_blocks):
        block = mr[b].astype(F32) * factor * fg_v[:, b * LANES : (b + 1) * LANES]
        big[b] = dot(placing, block.astype(BF16))

    def pack(dst):
        for pair in range(ep // 2):
            tile = big[:, pair * 8 : pair * 8 + 8, :].reshape(n_blocks // 2, 2, 8, LANES)
            even, odd = swap_halves(tile[:, 0], tile[:, 1])
            dst[2 * pair] = even.reshape(n_blocks * 4, LANES).astype(BF16)
            dst[2 * pair + 1] = odd.reshape(n_blocks * 4, LANES).astype(BF16)

    def unpack(src):
        for quad in range(ep // 4):
            halves = []
            for pair in (2 * quad, 2 * quad + 1):
                a = src[2 * pair].astype(F32).reshape(n_blocks // 2, 8, LANES)
                b = src[2 * pair + 1].astype(F32).reshape(n_blocks // 2, 8, LANES)
                halves.append(swap_halves(a, b))
            for odd in range(2):
                whole = jnp.concatenate([halves[0][odd], halves[1][odd]], axis=1).astype(BF16)
                for i in range(n_blocks // 2):
                    b = 2 * i + odd
                    xe[quad * 16 : quad * 16 + 16, b * LANES : (b + 1) * LANES] = whole[i]

    pack(ds_)
    dr[pl.ds(me_e, 1)] = ds_[pl.ds(me_e, 1)]
    send("ep", me_e, ep, CH_D, lambda j: ds_.at[j], dr)
    wait_all(ep, rsem.at[CH_D], dr)

    unpack(dr)
    both = dot(xe[...], wgu_v[...])
    kind = lax.div(lax.rem(lax.broadcasted_iota(jnp.int32, (n_slots, 1), 0), slots), CAP)
    parts = []
    for x in range(2):
        gate = both[:, 2 * x * hidden : (2 * x + 1) * hidden]
        upper = both[:, (2 * x + 1) * hidden : (2 * x + 2) * hidden]
        parts.append(jnp.where(kind == x, gate * jax.nn.sigmoid(gate) * upper, 0.0))
    hidden_rows = jnp.concatenate(parts, axis=1).astype(BF16)
    expert_rows = dot(hidden_rows, wd_v[...])
    for b in range(n_blocks):
        big[b] = expert_rows[:, b * LANES : (b + 1) * LANES]
    pack(rs)
    rr[pl.ds(me_e, 1)] = rs[pl.ds(me_e, 1)]
    send("ep", me_e, ep, CH_R, lambda j: rs.at[j], rr)
    wait_all(ep, rsem.at[CH_R], rr)

    unpack(rr)
    stacked = dot(combine_parts, xe[...])
    mix = stacked[:rows] + stacked[rows : 2 * rows] + stacked[2 * rows :]
    for j in range(tp):
        fs[j] = mix[:, j * cols : (j + 1) * cols].astype(BF16)
    fr[pl.ds(me_t, 1)] = fs[pl.ds(me_t, 1)]
    send("tp", me_t, tp, CH_F, lambda j: fs.at[j], fr)
    wait_all(tp, rsem.at[CH_F], fr)
    out_ref[...] = (mixed.astype(F32) + jnp.sum(fr[...].astype(F32), axis=0)).astype(BF16)

    for channel, n, buf in (
        (CH_X, ep, xs), (CH_Q, ep, qs), (CH_KV, ep, kvs), (CH_O, tp, os_),
        (CH_M, tp, mr), (CH_D, ep, ds_), (CH_R, ep, rs), (CH_F, tp, fs),
    ):
        wait_all(n, ssem.at[channel], buf)


def local(ep, tp, tokens, norm_gain, w_query, w_key, w_value, w_forget, forget_bias, query_gain,
          key_gain, cache_keys, cache_values, cache_gates, lengths, w_output, ffn_gain, routes,
          route_weights, w_gate, w_up, w_down):
    rows, width = tokens.shape
    span, hd = cache_keys.shape[2], cache_keys.shape[3]
    depth = w_query.shape[0]
    cols = width // tp
    hidden = w_gate.shape[2]
    heads = w_forget.shape[1]
    n_blocks = width // LANES
    packed = (ep, 2 * CAP * n_blocks, LANES)
    vmem = pltpu.VMEM
    scratch = [
        vmem((rows, width), BF16), vmem((1, width), F32), vmem((depth, 3 * hd), BF16),
        vmem((heads, width), BF16), vmem((1, heads), F32), vmem((1, hd), F32), vmem((1, hd), F32),
        vmem((rows, span, hd), BF16), vmem((rows, span, hd), BF16), vmem((rows, 1, span), F32),
        vmem((1, rows), jnp.int32), vmem((hd, width), BF16), vmem((1, width), F32),
        vmem((2, rows), jnp.int32), vmem((2, rows), F32), vmem((width, 4 * hidden), BF16),
        vmem((2 * hidden, width), BF16),
        vmem((ep, rows, depth), BF16), vmem((ep, rows, depth), BF16),
        vmem((ep, rows, hd), F32), vmem((ep, rows, hd), F32),
        vmem((ep, 2 * rows, hd), BF16), vmem((ep, 2 * rows, hd), BF16),
        vmem((tp, rows, cols), F32), vmem((tp, rows, cols), F32),
        vmem((rows, cols), BF16), vmem((tp, rows, cols), BF16),
        vmem(packed, BF16), vmem(packed, BF16), vmem(packed, BF16), vmem(packed, BF16),
        vmem((tp, rows, cols), BF16), vmem((tp, rows, cols), BF16),
        vmem((n_blocks, 2 * CAP * ep, LANES), F32), vmem((2 * CAP * ep, width), BF16),
        pltpu.SemaphoreType.DMA((32,)), pltpu.SemaphoreType.DMA((8,)),
        pltpu.SemaphoreType.DMA((8,)),
    ]
    operands = (
        tokens, norm_gain[None], w_query, w_key, w_value, w_forget.T, forget_bias[None],
        query_gain[None], key_gain[None], cache_keys, cache_values, cache_gates, lengths[None],
        w_output, ffn_gain[None], routes.T, route_weights.T, w_gate, w_up, w_down,
    )
    return pl.pallas_call(
        functools.partial(kernel, ep, tp),
        out_shape=jax.ShapeDtypeStruct((rows, cols), BF16),
        in_specs=[pl.BlockSpec(memory_space=pl.ANY)] * len(operands),
        out_specs=pl.BlockSpec(memory_space=pltpu.VMEM),
        scratch_shapes=scratch,
        compiler_params=pltpu.CompilerParams(
            collective_id=0, has_side_effects=True, vmem_limit_bytes=48 * 1024 * 1024
        ),
        name="layer",
    )(*operands)


def solution(mesh):
    placed = (
        P("ep", None), P(), P("ep", "tp"), P("ep", "tp"), P("ep", "tp"), P(), P(), P(), P(),
        P("ep", "tp", None, None), P("ep", "tp", None, None), P("ep", "tp", None), P("ep"),
        P("tp", None), P(), P("ep", None), P("ep", None), P("ep", None, "tp"),
        P("ep", None, "tp"), P("ep", "tp", None),
    )
    return jax.shard_map(
        functools.partial(local, mesh.shape["ep"], mesh.shape["tp"]),
        mesh=mesh, in_specs=placed, out_specs=P("ep", "tp"), check_vma=False,
    )
```

time: 128 us -> 68.7 us (0.54)
  Pallas kernels: 0 us -> 52.5 us
  waiting for transfers between devices: 41.7 us -> 0 us
  starting transfers between devices: 33.5 us -> 0 us
  blocking collectives: 26.3 us -> 0 us
  matrix products: 12.3 us -> 0 us
  local copies, waits for them, and re-layouts: 7.28 us -> 15.5 us
  other arithmetic: 6.01 us -> 0 us
    pallas_call x0 -> x1, Pallas kernels: none -> 52.5 us  [local(): pl.pallas_call(functools.partial(kernel, ep, tp), out_shape=jax.ShapeDtyp...]
    all_to_all x6 -> x0, waiting for transfers between devices: 41.7 us -> none  [the longest x2 14.8 us: sum_at_owner(): lax.all_to_all(cut_along(array, dim, length), axis, 0, 0, tiled=True)]
    all_to_all x6 -> x0, starting transfers between devices: 33.5 us -> none  [the longest x2 15 us: sum_at_owner(): lax.all_to_all(cut_along(array, dim, length), axis, 0, 0, tiled=True)]
    all_gather x1 -> x0, blocking collectives: 17.3 us -> none  [local(): arrived = lax.all_gather(arrived, 'tp', axis=3, tiled=True)]
    unnamed x19 -> x37, local copies, waits for them, and re-layouts: 0.81 us -> 15.5 us
    dot_general x12 -> x0, matrix products: 12.3 us -> none  [the longest x1 3.54 us: local(): jnp.einsum('bhd,bhld->bhl', queries, cache_keys, preferred_element_type=j...]
    all_to_all x1 -> x0, blocking collectives: 9.05 us -> none  [local(): lax.all_to_all(outgoing, 'ep', split_axis=0, concat_axis=0, tiled=True)]
    reduce_sum x13 -> x0, other arithmetic: 3.19 us -> none  [the longest x2 1.17 us: norm_rows(): jnp.mean(widened * widened, axis=-1, keepdims=True) + epsilon]
  transfers between devices with their start and end apart: 6 -> 0, of which waited for: 6 -> 0; matrix products, arithmetic and copies ran while one was open for 6% -> 0% of each run, Pallas kernels for 0% -> 0%
where the time goes in v1:
time: 68.7 us; the launch traced here: 68 us
  Pallas kernels  52.5 us (76%)
  local copies, waits for them, and re-layouts  15.5 us (23%)
    pallas_call x1, Pallas kernels, local(): pl.pallas_call(functools.partial(kernel, ep, tp), out_shape=jax.ShapeDtyp...  52.5 us
    unnamed x37, local copies, waits for them, and re-layouts  15.5 us

profile of v1, /device:TPU:1, one launch (start us, length us, event | category | flops | bytes accessed | tf_op | source)
XLA Modules:
  0.0 68.0 jit_solution(129413297016932807)
XLA Ops:
  0.0 0.0 copy-start
  0.0 1.2 %copy-done = bf16[2,2048,128]{2,1,0:T(8,128)(2,1)S(1)} copy-done((bf16[2,2048,128]{2,1,0:T(8,128)(2,1)S(1)}, bf16[2,2048,128]{2,1,0:T(8,128)(2,1)}, u32[]{:S(2)}) %copy-start) | copy-done | bytes 1048600
  1.2 0.0 copy-start.1
  1.2 1.2 %copy-done.1 = bf16[2,2048,128]{2,1,0:T(8,128)(2,1)S(1)} copy-done((bf16[2,2048,128]{2,1,0:T(8,128)(2,1)S(1)}, bf16[2,2048,128]{2,1,0:T(8,128)(2,1)}, u32[]{:S(2)}) %copy-start.1) | copy-done | bytes 1048600
  2.5 0.0 copy-start.2
  2.5 1.2 %copy-done.2 = bf16[2,128,2048]{2,1,0:T(8,128)(2,1)S(1)} copy-done((bf16[2,128,2048]{2,1,0:T(8,128)(2,1)S(1)}, bf16[2,128,2048]{2,1,0:T(8,128)(2,1)}, u32[]{:S(2)}) %copy-start.2) | copy-done | bytes 1048600
  3.7 0.0 copy-start.3
  3.7 1.0 %copy-done.3 = bf16[128,2048]{1,0:T(8,128)(2,1)S(1)} copy-done((bf16[128,2048]{1,0:T(8,128)(2,1)S(1)}, bf16[128,2048]{1,0:T(8,128)(2,1)}, u32[]{:S(2)}) %copy-start.3) | copy-done | bytes 524312
  4.7 0.0 copy-start.4
  4.7 0.8 %copy-done.4 = bf16[16,2048]{1,0:T(8,128)(2,1)S(1)} copy-done((bf16[16,2048]{1,0:T(8,128)(2,1)S(1)}, bf16[16,2048]{1,0:T(8,128)(2,1)}, u32[]{:S(2)}) %copy-start.4) | copy-done | bytes 65560
  5.6 0.0 copy-start.5
  5.6 0.8 %copy-done.5 = bf16[2048,16]{0,1:T(8,128)(2,1)S(1)} copy-done((bf16[2048,16]{0,1:T(8,128)(2,1)S(1)}, bf16[2048,16]{0,1:T(8,128)(2,1)}, u32[]{:S(2)}) %copy-start.5) | copy-done | bytes 65560
  6.4 0.0 copy-start.6
  6.4 0.8 %copy-done.6 = f32[16,1,1024]{2,1,0:T(1,128)S(1)} copy-done((f32[16,1,1024]{2,1,0:T(1,128)S(1)}, f32[16,1,1024]{2,1,0:T(1,128)}, u32[]{:S(2)}) %copy-start.6) | copy-done | bytes 65560
  7.2 0.0 copy-start.7
  7.2 0.8 %copy-done.7 = bf16[128,128]{1,0:T(8,128)(2,1)S(1)} copy-done((bf16[128,128]{1,0:T(8,128)(2,1)S(1)}, bf16[128,128]{1,0:T(8,128)(2,1)}, u32[]{:S(2)}) %copy-start.7) | copy-done | bytes 32792
  8.0 0.0 copy-start.8
  8.0 0.8 %copy-done.8 = bf16[128,128]{1,0:T(8,128)(2,1)S(1)} copy-done((bf16[128,128]{1,0:T(8,128)(2,1)S(1)}, bf16[128,128]{1,0:T(8,128)(2,1)}, u32[]{:S(2)}) %copy-start.8) | copy-done | bytes 32792
  8.8 0.0 copy-start.9
  8.8 0.8 %copy-done.9 = bf16[128,128]{1,0:T(8,128)(2,1)S(1)} copy-done((bf16[128,128]{1,0:T(8,128)(2,1)S(1)}, bf16[128,128]{1,0:T(8,128)(2,1)}, u32[]{:S(2)}) %copy-start.9) | copy-done | bytes 32792
  9.5 0.0 copy-start.10
  9.5 0.7 %copy-done.10 = f32[2048]{0:T(1024)S(1)} copy-done((f32[2048]{0:T(1024)S(1)}, f32[2048]{0:T(1024)}, u32[]{:S(2)}) %copy-start.10) | copy-done | bytes 8216
  10.2 0.0 copy-start.11
  10.2 0.7 %copy-done.11 = f32[2048]{0:T(1024)S(1)} copy-done((f32[2048]{0:T(1024)S(1)}, f32[2048]{0:T(1024)}, u32[]{:S(2)}) %copy-start.11) | copy-done | bytes 8216
  10.9 0.7 copy-done.12
  11.6 0.7 copy-done.13
  12.3 0.7 copy-done.14
  12.9 0.7 copy-done.15
  13.6 0.7 copy-done.16
  14.2 0.7 copy-done.17
  14.9 52.5 %layer.1 = bf16[16,128]{1,0:T(8,128)(2,1)S(1)} custom-call(bf16[16,2048]{1,0:T(8,128)(2,1)S(1)} %copy-done.4, f32[1,2048]{1,0:T(1,128)S(1)} %bitcast.10, bf16[128,128]{1,0:T(8,128)(2,1)S(1)} %copy-done.7, bf16[128,128]{1,0:T(8,128)(2,1)S(1)} %copy-done.8, bf16[128,128]{1,0:T(8,128)(2,1)S(1)} %copy-done.9, bf16[16,2048]{1,0:T(8,128)(2,1)S(1)} %bitcast.9, ...), custom_call_target="tpu_custom_call" | custom-call | tf_op jit(solution)/shard_map/layer/pallas_call | solution.py:366
  67.4 0.6 copy.22
  (6 shorter events, 0.0 us)
Async XLA Ops:
  0.0 1.2 %copy-start = (bf16[2,2048,128]{2,1,0:T(8,128)(2,1)S(1)}, bf16[2,2048,128]{2,1,0:T(8,128)(2,1)}, u32[]{:S(2)}) copy-start(bf16[2,2048,128]{2,1,0:T(8,128)(2,1)} %refs_17_.1) | copy-start | bytes 3145732
  1.2 1.2 %copy-start.1 = (bf16[2,2048,128]{2,1,0:T(8,128)(2,1)S(1)}, bf16[2,2048,128]{2,1,0:T(8,128)(2,1)}, u32[]{:S(2)}) copy-start(bf16[2,2048,128]{2,1,0:T(8,128)(2,1)} %refs_18_.1) | copy-start | bytes 3145732
  2.5 1.2 %copy-start.2 = (bf16[2,128,2048]{2,1,0:T(8,128)(2,1)S(1)}, bf16[2,128,2048]{2,1,0:T(8,128)(2,1)}, u32[]{:S(2)}) copy-start(bf16[2,128,2048]{2,1,0:T(8,128)(2,1)} %refs_19_.1) | copy-start | bytes 3145732
  3.7 1.0 %copy-start.3 = (bf16[128,2048]{1,0:T(8,128)(2,1)S(1)}, bf16[128,2048]{1,0:T(8,128)(2,1)}, u32[]{:S(2)}) copy-start(bf16[128,2048]{1,0:T(8,128)(2,1)} %refs_13_.1) | copy-start | bytes 1572868
  4.7 0.8 %copy-start.4 = (bf16[16,2048]{1,0:T(8,128)(2,1)S(1)}, bf16[16,2048]{1,0:T(8,128)(2,1)}, u32[]{:S(2)}) copy-start(bf16[16,2048]{1,0:T(8,128)(2,1)} %refs_0_.1) | copy-start | bytes 196612
  5.6 0.8 %copy-start.5 = (bf16[2048,16]{0,1:T(8,128)(2,1)S(1)}, bf16[2048,16]{0,1:T(8,128)(2,1)}, u32[]{:S(2)}) copy-start(bf16[2048,16]{0,1:T(8,128)(2,1)} %param.25) | copy-start | bytes 196612
  6.4 0.8 %copy-start.6 = (f32[16,1,1024]{2,1,0:T(1,128)S(1)}, f32[16,1,1024]{2,1,0:T(1,128)}, u32[]{:S(2)}) copy-start(f32[16,1,1024]{2,1,0:T(1,128)} %refs_11_.1) | copy-start | bytes 196612
  7.2 0.8 %copy-start.7 = (bf16[128,128]{1,0:T(8,128)(2,1)S(1)}, bf16[128,128]{1,0:T(8,128)(2,1)}, u32[]{:S(2)}) copy-start(bf16[128,128]{1,0:T(8,128)(2,1)} %refs_2_.1) | copy-start | bytes 98308
  8.0 0.8 %copy-start.8 = (bf16[128,128]{1,0:T(8,128)(2,1)S(1)}, bf16[128,128]{1,0:T(8,128)(2,1)}, u32[]{:S(2)}) copy-start(bf16[128,128]{1,0:T(8,128)(2,1)} %refs_3_.1) | copy-start | bytes 98308
  8.8 0.8 %copy-start.9 = (bf16[128,128]{1,0:T(8,128)(2,1)S(1)}, bf16[128,128]{1,0:T(8,128)(2,1)}, u32[]{:S(2)}) copy-start(bf16[128,128]{1,0:T(8,128)(2,1)} %refs_4_.1) | copy-start | bytes 98308
  9.5 0.7 %copy-start.10 = (f32[2048]{0:T(1024)S(1)}, f32[2048]{0:T(1024)}, u32[]{:S(2)}) copy-start(f32[2048]{0:T(1024)} %param.21) | copy-start | bytes 24580
  10.2 0.7 %copy-start.11 = (f32[2048]{0:T(1024)S(1)}, f32[2048]{0:T(1024)}, u32[]{:S(2)}) copy-start(f32[2048]{0:T(1024)} %param.34) | copy-start | bytes 24580
  10.9 0.7 copy-start.12
  11.6 0.7 copy-start.13
  12.3 0.7 copy-start.14
  12.9 0.7 copy-start.15
  13.6 0.7 copy-start.16
  14.2 0.7 copy-start.17

commit v2 on v1

--- a/solution.py
+++ b/solution.py
@@ -33,6 +33,18 @@
     low = lax.broadcasted_iota(jnp.int32, a.shape, 1) < 4
     a_turned, b_turned = pltpu.roll(a, 4, 1), pltpu.roll(b, 4, 1)
     return jnp.where(low, a, b_turned), jnp.where(low, a_turned, b)
+
+
+def far_first(me, outer, inner):
+    def hops(step):
+        return min(step[0], outer - step[0]) + min(step[1], inner - step[1])
+
+    steps = [(a, b) for a in range(outer) for b in range(inner) if a or b]
+    a_me, b_me = lax.div(me, inner), lax.rem(me, inner)
+    return [
+        lax.rem(a_me + a, outer) * inner + lax.rem(b_me + b, inner)
+        for a, b in sorted(steps, key=lambda step: -hops(step))
+    ]
 
 
 def kernel(ep, tp, *refs):
@@ -58,6 +70,12 @@
     slots = 2 * CAP
     n_slots = ep * slots
 
+    peers = {"ep": far_first(me_e, ep // 4, 4), "tp": far_first(me_t, tp // 2, 2)}
+    barrier = pltpu.get_barrier_semaphore()
+    for axis in ("ep", "tp"):
+        for peer in peers[axis]:
+            pl.semaphore_signal(barrier, inc=1, device_id={axis: peer}, device_id_type=MESH)
+
     fetches = {}
 
     def fetch(name, pairs):
@@ -107,23 +125,9 @@
     )
     fetch("wd", [(hbm["wd"].at[x], wd_v.at[pl.ds(x * hidden, hidden)]) for x in range(2)])
 
-    barrier = pltpu.get_barrier_semaphore()
-
-    def greet(axis, me, n):
-        def body(i, carry):
-            pl.semaphore_signal(
-                barrier, inc=1, device_id={axis: lax.rem(me + i, n)}, device_id_type=MESH
-            )
-            return carry
-
-        lax.fori_loop(1, n, body, 0)
-
-    greet("ep", me_e, ep)
-    greet("tp", me_t, tp)
-
-    def send(axis, me, n, channel, src, dst):
-        def body(i, carry):
-            peer = lax.rem(me + i, n)
+    def send(axis, channel, src, dst):
+        me = lax.axis_index(axis)
+        for peer in peers[axis]:
             pltpu.make_async_remote_copy(
                 src_ref=src(peer),
                 dst_ref=dst.at[me],
@@ -132,9 +136,6 @@
                 device_id={axis: peer},
                 device_id_type=MESH,
             ).start()
-            return carry
-
-        lax.fori_loop(1, n, body, 0)
 
     def wait_all(n, sem, buf):
         part = buf.at[pl.ds(0, n - 1)]
@@ -146,7 +147,7 @@
         xs[j] = normed[:, j * depth : (j + 1) * depth]
     xr[pl.ds(me_e, 1)] = xs[pl.ds(me_e, 1)]
     pl.semaphore_wait(barrier, ep + tp - 2)
-    send("ep", me_e, ep, CH_X, lambda j: xs.at[j], xr)
+    send("ep", CH_X, lambda j: xs.at[j], xr)
 
     need("small")
     row = lax.broadcasted_iota(jnp.int32, (rows, 1), 0)
@@ -213,8 +214,8 @@
         kvs[j, rows : 2 * rows, :] = own[:, 2 * hd :].astype(BF16)
     qr[pl.ds(me_e, 1)] = qs[pl.ds(me_e, 1)]
     kvr[pl.ds(me_e, 1)] = kvs[pl.ds(me_e, 1)]
-    send("ep", me_e, ep, CH_Q, lambda j: qs.at[j], qr)
-    send("ep", me_e, ep, CH_KV, lambda j: kvs.at[j], kvr)
+    send("ep", CH_Q, lambda j: qs.at[j], qr)
+    send("ep", CH_KV, lambda j: kvs.at[j], kvr)
     need("k", "v")
     wait_all(ep, rsem.at[CH_Q], qr)
     queries = norm(jnp.sum(qr[...], axis=0), qg_v[...]).astype(BF16)
@@ -248,15 +249,15 @@
     cols = or_.shape[2]
     partial = dot(attended, wo_v[...])
     for j in range(tp):
-        os_[j] = partial[:, j * cols : (j + 1) * cols]
+        os_[j] = partial[:, j * cols : (j + 1) * cols].astype(BF16)
     or_[pl.ds(me_t, 1)] = os_[pl.ds(me_t, 1)]
-    send("tp", me_t, tp, CH_O, lambda j: os_.at[j], or_)
+    send("tp", CH_O, lambda j: os_.at[j], or_)
     wait_all(tp, rsem.at[CH_O], or_)
     own_tokens = tok_v[:, pl.ds(pl.multiple_of(me_t * cols, cols), cols)].astype(F32)
-    mixed = (own_tokens + jnp.sum(or_[...], axis=0)).astype(BF16)
+    mixed = (own_tokens + jnp.sum(or_[...].astype(F32), axis=0)).astype(BF16)
     ms[...] = mixed
     mr[pl.ds(me_t, 1)] = mixed[None]
-    send("tp", me_t, tp, CH_M, lambda j: ms, mr)
+    send("tp", CH_M, lambda j: ms, mr)
     need("wgu", "wd")
     wait_all(tp, rsem.at[CH_M], mr)
 
@@ -291,7 +292,7 @@
 
     pack(ds_)
     dr[pl.ds(me_e, 1)] = ds_[pl.ds(me_e, 1)]
-    send("ep", me_e, ep, CH_D, lambda j: ds_.at[j], dr)
+    send("ep", CH_D, lambda j: ds_.at[j], dr)
     wait_all(ep, rsem.at[CH_D], dr)
 
     unpack(dr)
@@ -308,7 +309,7 @@
         big[b] = expert_rows[:, b * LANES : (b + 1) * LANES]
     pack(rs)
     rr[pl.ds(me_e, 1)] = rs[pl.ds(me_e, 1)]
-    send("ep", me_e, ep, CH_R, lambda j: rs.at[j], rr)
+    send("ep", CH_R, lambda j: rs.at[j], rr)
     wait_all(ep, rsem.at[CH_R], rr)
 
     unpack(rr)
@@ -317,7 +318,7 @@
     for j in range(tp):
         fs[j] = mix[:, j * cols : (j + 1) * cols].astype(BF16)
     fr[pl.ds(me_t, 1)] = fs[pl.ds(me_t, 1)]
-    send("tp", me_t, tp, CH_F, lambda j: fs.at[j], fr)
+    send("tp", CH_F, lambda j: fs.at[j], fr)
     wait_all(tp, rsem.at[CH_F], fr)
     out_ref[...] = (mixed.astype(F32) + jnp.sum(fr[...].astype(F32), axis=0)).astype(BF16)
 
@@ -350,7 +351,7 @@
         vmem((ep, rows, depth), BF16), vmem((ep, rows, depth), BF16),
         vmem((ep, rows, hd), F32), vmem((ep, rows, hd), F32),
         vmem((ep, 2 * rows, hd), BF16), vmem((ep, 2 * rows, hd), BF16),
-        vmem((tp, rows, cols), F32), vmem((tp, rows, cols), F32),
+        vmem((tp, rows, cols), BF16), vmem((tp, rows, cols), BF16),
         vmem((rows, cols), BF16), vmem((tp, rows, cols), BF16),
         vmem(packed, BF16), vmem(packed, BF16), vmem(packed, BF16), vmem(packed, BF16),
         vmem((tp, rows, cols), BF16), vmem((tp, rows, cols), BF16),
@@ -366,11 +367,11 @@
     return pl.pallas_call(
         functools.partial(kernel, ep, tp),
         out_shape=jax.ShapeDtypeStruct((rows, cols), BF16),
-        in_specs=[pl.BlockSpec(memory_space=pl.ANY)] * len(operands),
+        in_specs=[pl.BlockSpec(memory_space=pltpu.HBM)] * len(operands),
         out_specs=pl.BlockSpec(memory_space=pltpu.VMEM),
         scratch_shapes=scratch,
         compiler_params=pltpu.CompilerParams(
-            collective_id=0, has_side_effects=True, vmem_limit_bytes=48 * 1024 * 1024
+            collective_id=0, has_side_effects=True, vmem_limit_bytes=67043328
         ),
         name="layer",
     )(*operands)

time: 68.7 us -> 51 us (0.74)
  local copies, waits for them, and re-layouts: 15.5 us -> 1.28 us
  Pallas kernels: 52.5 us -> 49.6 us
    unnamed x37 -> x1, local copies, waits for them, and re-layouts: 15.5 us -> 1.28 us
    pallas_call x1, Pallas kernels: 52.5 us -> 49.6 us  [local(): pl.pallas_call(functools.partial(kernel, ep, tp), out_shape=jax.ShapeDtyp...]
where the time goes in v2:
time: 51 us; the launch traced here: 50.9 us
  Pallas kernels  49.6 us (97%)
  local copies, waits for them, and re-layouts  1.28 us (3%)
    pallas_call x1, Pallas kernels, local(): pl.pallas_call(functools.partial(kernel, ep, tp), out_shape=jax.ShapeDtyp...  49.6 us
    unnamed x1, local copies, waits for them, and re-layouts  1.28 us

profile of v2, /device:TPU:1, one launch (start us, length us, event | category | flops | bytes accessed | tf_op | source)
XLA Modules:
  0.0 50.9 jit_solution(6778495720696420649)
XLA Ops:
  0.0 49.6 %layer.1 = bf16[16,128]{1,0:T(8,128)(2,1)} custom-call(bf16[16,2048]{1,0:T(8,128)(2,1)} %refs_0_.1, f32[1,2048]{1,0:T(1,128)} %bitcast.10, bf16[128,128]{1,0:T(8,128)(2,1)} %refs_2_.1, bf16[128,128]{1,0:T(8,128)(2,1)} %refs_3_.1, bf16[128,128]{1,0:T(8,128)(2,1)} %refs_4_.1, bf16[16,2048]{1,0:T(8,128)(2,1)} %bitcast.9, f32[1,16]{1,0:T(1,128)} %bitcast.14, ...), custom_call_target="tpu_custom_call" | custom-call | tf_op jit(solution)/shard_map/layer/pallas_call | solution.py:367
  49.6 1.3 %copy.22 = bf16[16,128]{1,0:T(8,128)(2,1)} copy(bf16[16,128]{1,0:T(8,128)(2,1)} %layer.1) | data formatting | bytes 8192

commit v3 on v2

--- a/solution.py
+++ b/solution.py
@@ -1,4 +1,5 @@
 import functools
+import itertools
 
 import jax
 import jax.numpy as jnp
@@ -14,7 +15,7 @@
 CAP = 2
 LANES = 128
 
-CH_X, CH_Q, CH_KV, CH_O, CH_M, CH_D, CH_R, CH_F = range(8)
+CH_X, CH_Q, CH_KV, CH_O, CH_D, CH_DP, CH_RP, CH_R = range(8)
 
 
 def norm(v, gain):
@@ -29,22 +30,14 @@
     return lax.dot_general(a, b, (((1,), (1,)), ((), ())), preferred_element_type=F32)
 
 
-def swap_halves(a, b):
-    low = lax.broadcasted_iota(jnp.int32, a.shape, 1) < 4
-    a_turned, b_turned = pltpu.roll(a, 4, 1), pltpu.roll(b, 4, 1)
-    return jnp.where(low, a, b_turned), jnp.where(low, a_turned, b)
-
-
-def far_first(me, outer, inner):
-    def hops(step):
-        return min(step[0], outer - step[0]) + min(step[1], inner - step[1])
-
-    steps = [(a, b) for a in range(outer) for b in range(inner) if a or b]
-    a_me, b_me = lax.div(me, inner), lax.rem(me, inner)
-    return [
-        lax.rem(a_me + a, outer) * inner + lax.rem(b_me + b, inner)
-        for a, b in sorted(steps, key=lambda step: -hops(step))
-    ]
+def far_first(*sizes):
+    steps = itertools.product(*(range(size) for size in sizes))
+    steps = sorted(steps, key=lambda step: -sum(min(a, n - a) for a, n in zip(step, sizes)))
+    return steps[:-1]
+
+
+def moved(me, size, step):
+    return lax.rem(me + step, size) if step else me
 
 
 def kernel(ep, tp, *refs):
@@ -57,20 +50,28 @@
     (
         tok_v, ng_v, wqkv_v, wf_v, fb_v, qg_v, kg_v, k_v, v_v, g_v, len_v,
         wo_v, fg_v, rt_v, rw_v, wgu_v, wd_v,
-        xs, xr, qs, qr, kvs, kvr, os_, or_, ms, mr, ds_, dr, rs, rr, fs, fr,
-        big, xe,
+        xs, xr, qs, qr, kvs, kvr, os_, or_, ds_, dr, dw, dp, rg, rp, rs, rr, big, xe,
         hsem, ssem, rsem,
     ) = refs[len(names) + 1 :]
 
     me_e, me_t = lax.axis_index("ep"), lax.axis_index("tp")
     rows, width = tok_v.shape
-    span, hd = k_v.shape[1], k_v.shape[2]
-    n_blocks = width // LANES
+    span, hd = k_v.shape[1], k_v.shape[2] // 2
     depth = xs.shape[2]
     slots = 2 * CAP
     n_slots = ep * slots
 
-    peers = {"ep": far_first(me_e, ep // 4, 4), "tp": far_first(me_t, tp // 2, 2)}
+    outer, chips = ep // 4, tp // 2
+    y, x = lax.div(me_e, 4), lax.rem(me_e, 4)
+    z, core = lax.div(me_t, 2), lax.rem(me_t, 2)
+    y_at = [moved(y, outer, a) for a in range(outer)]
+    x_at = [moved(x, 4, a) for a in range(4)]
+    z_at = [moved(z, chips, a) for a in range(chips)]
+    core_at = [core, 1 - core]
+    peers = {
+        "ep": [y_at[a] * 4 + x_at[b] for a, b in far_first(outer, 4)],
+        "tp": [z_at[a] * 2 + core_at[b] for a, b in far_first(chips, 2)],
+    }
     barrier = pltpu.get_barrier_semaphore()
     for axis in ("ep", "tp"):
         for peer in peers[axis]:
@@ -104,15 +105,14 @@
             (hbm["ffn_gain"], fg_v), (hbm["routes"], rt_v), (hbm["r_weights"], rw_v),
         ],
     )
-    quarter = rows // 4
-    fetch(
-        "k",
-        [(hbm["keys"].at[pl.ds(i * quarter, quarter), 0], k_v.at[pl.ds(i * quarter, quarter)]) for i in range(4)],
-    )
-    fetch(
-        "v",
-        [(hbm["values"].at[pl.ds(i * quarter, quarter), 0], v_v.at[pl.ds(i * quarter, quarter)]) for i in range(4)],
-    )
+    for name, src, dst in (("k", "keys", k_v), ("v", "values", v_v)):
+        fetch(
+            name,
+            [
+                (hbm[src].at[s, 0], dst.at[s // 2, :, pl.ds((s % 2) * hd, hd)])
+                for s in range(rows)
+            ],
+        )
     fetch("wo", [(hbm["wo"], wo_v)])
     hidden = hbm["wg"].shape[2]
     fetch(
@@ -221,9 +221,11 @@
     queries = norm(jnp.sum(qr[...], axis=0), qg_v[...]).astype(BF16)
 
     score_scale = hd ** (-0.5)
+    wide = queries.astype(F32)
     scores = jnp.zeros((rows, span), F32)
-    for s in range(rows):
-        scores = jnp.where(row == s, dot_t(queries, k_v[s]), scores)
+    for pair in range(rows // 2):
+        both = [jnp.where(row == 2 * pair + i, wide, 0.0) for i in range(2)]
+        scores = scores + dot_t(jnp.concatenate(both, axis=1).astype(BF16), k_v[pair])
     wait_all(ep, rsem.at[CH_KV], kvr)
     kv_raw = jnp.sum(kvr[...].astype(F32), axis=0)
     keys_new = norm(kv_raw[:rows], kg_v[...]).astype(BF16)
@@ -239,11 +241,12 @@
     denominator = jnp.sum(weights, axis=1, keepdims=True) + own_weight
     probabilities = weights / denominator
     own_prob = (own_weight / denominator).astype(BF16).astype(F32)
-    attended = own_prob * values_new.astype(F32)
-    for s in range(rows):
-        mine = jnp.where(row == s, probabilities, 0.0).astype(BF16)
-        attended = attended + dot(mine, v_v[s])
-    attended = attended.astype(BF16)
+    summed = jnp.zeros((rows, 2 * hd), F32)
+    for pair in range(rows // 2):
+        mine = jnp.where(lax.div(row, 2) == pair, probabilities, 0.0).astype(BF16)
+        summed = summed + dot(mine, v_v[pair])
+    summed = jnp.where(lax.rem(row, 2) == 0, summed[:, :hd], summed[:, hd:])
+    attended = (summed + own_prob * values_new.astype(F32)).astype(BF16)
 
     need("wo")
     cols = or_.shape[2]
@@ -255,78 +258,104 @@
     wait_all(tp, rsem.at[CH_O], or_)
     own_tokens = tok_v[:, pl.ds(pl.multiple_of(me_t * cols, cols), cols)].astype(F32)
     mixed = (own_tokens + jnp.sum(or_[...].astype(F32), axis=0)).astype(BF16)
-    ms[...] = mixed
-    mr[pl.ds(me_t, 1)] = mixed[None]
-    send("tp", CH_M, lambda j: ms, mr)
+
+    def send_grid(channel, src, dst):
+        for a, b, d in far_first(outer, 4, chips):
+            owner = y_at[a] * 4 + x_at[b]
+            pltpu.make_async_remote_copy(
+                src_ref=src(owner, z_at[d]),
+                dst_ref=dst.at[pl.ds(z * n_slots + slots * me_e, slots)],
+                send_sem=ssem.at[channel],
+                recv_sem=rsem.at[channel],
+                device_id={"ep": owner, "tp": z_at[d] * 2 + core},
+                device_id_type=MESH,
+            ).start()
+
+    def wait_grid(sem, buf):
+        part = buf.at[pl.ds(0, (ep * chips - 1) * slots)]
+        pltpu.make_async_copy(part, part, sem).wait()
+
+    def to_partner(channel, src, dst):
+        copy = pltpu.make_async_remote_copy(
+            src_ref=src,
+            dst_ref=dst,
+            send_sem=ssem.at[channel],
+            recv_sem=rsem.at[channel],
+            device_id={"tp": z * 2 + 1 - core},
+            device_id_type=MESH,
+        )
+        copy.start()
+        return copy
+
+    slot_line = lax.broadcasted_iota(jnp.int32, (n_slots, 1), 0)
+    own_slots = lax.div(slot_line, slots) == me_e
+
+    def part_of(buf, own, chip):
+        got = buf[chip * n_slots : (chip + 1) * n_slots, :].astype(F32)
+        return jnp.where(own_slots & (z == chip), own, got)
+
+    placed = dot(placing, mixed)
+    ds_[...] = placed.astype(BF16)
+    send_grid(CH_D, lambda owner, chip: ds_.at[pl.ds(slots * owner, slots)], dr)
     need("wgu", "wd")
-    wait_all(tp, rsem.at[CH_M], mr)
-
-    squares = jnp.zeros((rows, 1), F32)
-    for b in range(n_blocks):
-        block = mr[b].astype(F32)
-        squares = squares + jnp.sum(block * block, axis=1, keepdims=True)
-    factor = lax.rsqrt(squares / width + EPS)
-    for b in range(n_blocks):
-        block = mr[b].astype(F32) * factor * fg_v[:, b * LANES : (b + 1) * LANES]
-        big[b] = dot(placing, block.astype(BF16))
-
-    def pack(dst):
-        for pair in range(ep // 2):
-            tile = big[:, pair * 8 : pair * 8 + 8, :].reshape(n_blocks // 2, 2, 8, LANES)
-            even, odd = swap_halves(tile[:, 0], tile[:, 1])
-            dst[2 * pair] = even.reshape(n_blocks * 4, LANES).astype(BF16)
-            dst[2 * pair + 1] = odd.reshape(n_blocks * 4, LANES).astype(BF16)
-
-    def unpack(src):
-        for quad in range(ep // 4):
-            halves = []
-            for pair in (2 * quad, 2 * quad + 1):
-                a = src[2 * pair].astype(F32).reshape(n_blocks // 2, 8, LANES)
-                b = src[2 * pair + 1].astype(F32).reshape(n_blocks // 2, 8, LANES)
-                halves.append(swap_halves(a, b))
-            for odd in range(2):
-                whole = jnp.concatenate([halves[0][odd], halves[1][odd]], axis=1).astype(BF16)
-                for i in range(n_blocks // 2):
-                    b = 2 * i + odd
-                    xe[quad * 16 : quad * 16 + 16, b * LANES : (b + 1) * LANES] = whole[i]
-
-    pack(ds_)
-    dr[pl.ds(me_e, 1)] = ds_[pl.ds(me_e, 1)]
-    send("ep", CH_D, lambda j: ds_.at[j], dr)
-    wait_all(ep, rsem.at[CH_D], dr)
-
-    unpack(dr)
+    wait_grid(rsem.at[CH_D], dr)
+    squares = jnp.zeros((n_slots, LANES), F32)
+    for chip in range(chips):
+        block = part_of(dr, placed, chip)
+        squares = squares + block * block
+        dw[chip * n_slots : (chip + 1) * n_slots, :] = block.astype(BF16)
+    swap = to_partner(CH_DP, dw, dp)
+    swap.wait_recv()
+    for chip in range(chips):
+        block = dp[chip * n_slots : (chip + 1) * n_slots, :].astype(F32)
+        squares = squares + block * block
+    factor = lax.rsqrt(jnp.sum(squares, axis=1, keepdims=True) / width + EPS)
+    for buf, owner in ((dw, core), (dp, 1 - core)):
+        for chip in range(chips):
+            at = pl.multiple_of((2 * chip + owner) * LANES, LANES)
+            block = buf[chip * n_slots : (chip + 1) * n_slots, :].astype(F32)
+            block = block * factor * fg_v[:, pl.ds(at, LANES)]
+            xe[:, pl.ds(at, LANES)] = block.astype(BF16)
+
     both = dot(xe[...], wgu_v[...])
-    kind = lax.div(lax.rem(lax.broadcasted_iota(jnp.int32, (n_slots, 1), 0), slots), CAP)
+    kind = lax.div(lax.rem(slot_line, slots), CAP)
     parts = []
-    for x in range(2):
-        gate = both[:, 2 * x * hidden : (2 * x + 1) * hidden]
-        upper = both[:, (2 * x + 1) * hidden : (2 * x + 2) * hidden]
-        parts.append(jnp.where(kind == x, gate * jax.nn.sigmoid(gate) * upper, 0.0))
+    for i in range(2):
+        gate = both[:, 2 * i * hidden : (2 * i + 1) * hidden]
+        upper = both[:, (2 * i + 1) * hidden : (2 * i + 2) * hidden]
+        parts.append(jnp.where(kind == i, gate * jax.nn.sigmoid(gate) * upper, 0.0))
     hidden_rows = jnp.concatenate(parts, axis=1).astype(BF16)
-    expert_rows = dot(hidden_rows, wd_v[...])
-    for b in range(n_blocks):
-        big[b] = expert_rows[:, b * LANES : (b + 1) * LANES]
-    pack(rs)
-    rr[pl.ds(me_e, 1)] = rs[pl.ds(me_e, 1)]
-    send("ep", CH_R, lambda j: rs.at[j], rr)
-    wait_all(ep, rsem.at[CH_R], rr)
-
-    unpack(rr)
-    stacked = dot(combine_parts, xe[...])
+
+    def down(chip, owner):
+        at = pl.multiple_of((2 * chip + owner) * LANES, LANES)
+        return dot(hidden_rows, wd_v[:, pl.ds(at, LANES)])
+
+    for chip in range(chips):
+        rg[chip * n_slots : (chip + 1) * n_slots, :] = down(chip, 1 - core).astype(BF16)
+    give = to_partner(CH_RP, rg, rp)
+    for chip in range(chips):
+        big[chip * n_slots : (chip + 1) * n_slots, :] = down(chip, core)
+    give.wait_recv()
+    for chip in range(chips):
+        at = slice(chip * n_slots, (chip + 1) * n_slots)
+        rs[at, :] = (big[at, :] + rp[at, :].astype(F32)).astype(BF16)
+    send_grid(CH_R, lambda owner, chip: rs.at[pl.ds(chip * n_slots + slots * owner, slots)], rr)
+    wait_grid(rsem.at[CH_R], rr)
+
+    own_rows = rs[pl.ds(pl.multiple_of(z * n_slots, n_slots), n_slots), :].astype(F32)
+    total = jnp.zeros((n_slots, LANES), F32)
+    for chip in range(chips):
+        total = total + part_of(rr, own_rows, chip)
+    stacked = dot(combine_parts, total.astype(BF16))
     mix = stacked[:rows] + stacked[rows : 2 * rows] + stacked[2 * rows :]
-    for j in range(tp):
-        fs[j] = mix[:, j * cols : (j + 1) * cols].astype(BF16)
-    fr[pl.ds(me_t, 1)] = fs[pl.ds(me_t, 1)]
-    send("tp", CH_F, lambda j: fs.at[j], fr)
-    wait_all(tp, rsem.at[CH_F], fr)
-    out_ref[...] = (mixed.astype(F32) + jnp.sum(fr[...].astype(F32), axis=0)).astype(BF16)
-
-    for channel, n, buf in (
-        (CH_X, ep, xs), (CH_Q, ep, qs), (CH_KV, ep, kvs), (CH_O, tp, os_),
-        (CH_M, tp, mr), (CH_D, ep, ds_), (CH_R, ep, rs), (CH_F, tp, fs),
-    ):
+    out_ref[...] = (mixed.astype(F32) + mix).astype(BF16)
+
+    for channel, n, buf in ((CH_X, ep, xs), (CH_Q, ep, qs), (CH_KV, ep, kvs), (CH_O, tp, os_)):
         wait_all(n, ssem.at[channel], buf)
+    for channel, buf in ((CH_D, dr), (CH_R, rs)):
+        wait_grid(ssem.at[channel], buf)
+    swap.wait_send()
+    give.wait_send()
 
 
 def local(ep, tp, tokens, norm_gain, w_query, w_key, w_value, w_forget, forget_bias, query_gain,
@@ -338,13 +367,12 @@
     cols = width // tp
     hidden = w_gate.shape[2]
     heads = w_forget.shape[1]
-    n_blocks = width // LANES
-    packed = (ep, 2 * CAP * n_blocks, LANES)
+    n_slots = 2 * CAP * ep
     vmem = pltpu.VMEM
     scratch = [
         vmem((rows, width), BF16), vmem((1, width), F32), vmem((depth, 3 * hd), BF16),
         vmem((heads, width), BF16), vmem((1, heads), F32), vmem((1, hd), F32), vmem((1, hd), F32),
-        vmem((rows, span, hd), BF16), vmem((rows, span, hd), BF16), vmem((rows, 1, span), F32),
+        vmem((rows // 2, span, 2 * hd), BF16), vmem((rows // 2, span, 2 * hd), BF16), vmem((rows, 1, span), F32),
         vmem((1, rows), jnp.int32), vmem((hd, width), BF16), vmem((1, width), F32),
         vmem((2, rows), jnp.int32), vmem((2, rows), F32), vmem((width, 4 * hidden), BF16),
         vmem((2 * hidden, width), BF16),
@@ -352,11 +380,9 @@
         vmem((ep, rows, hd), F32), vmem((ep, rows, hd), F32),
         vmem((ep, 2 * rows, hd), BF16), vmem((ep, 2 * rows, hd), BF16),
         vmem((tp, rows, cols), BF16), vmem((tp, rows, cols), BF16),
-        vmem((rows, cols), BF16), vmem((tp, rows, cols), BF16),
-        vmem(packed, BF16), vmem(packed, BF16), vmem(packed, BF16), vmem(packed, BF16),
-        vmem((tp, rows, cols), BF16), vmem((tp, rows, cols), BF16),
-        vmem((n_blocks, 2 * CAP * ep, LANES), F32), vmem((2 * CAP * ep, width), BF16),
-        pltpu.SemaphoreType.DMA((32,)), pltpu.SemaphoreType.DMA((8,)),
+        vmem((n_slots, LANES), BF16), *[vmem((tp // 2 * n_slots, LANES), BF16)] * 7,
+        vmem((tp // 2 * n_slots, LANES), F32), vmem((n_slots, width), BF16),
+        pltpu.SemaphoreType.DMA((64,)), pltpu.SemaphoreType.DMA((8,)),
         pltpu.SemaphoreType.DMA((8,)),
     ]
     operands = (

time: 51 us -> 46.8 us (0.918)
  Pallas kernels: 49.6 us -> 45.4 us
    pallas_call x1, Pallas kernels: 49.6 us -> 45.4 us  [local(): pl.pallas_call(functools.partial(kernel, ep, tp), out_shape=jax.ShapeDtyp...]
where the time goes in v3:
time: 46.8 us; the launch traced here: 46.6 us
  Pallas kernels  45.4 us (97%)
  local copies, waits for them, and re-layouts  1.28 us (3%)
    pallas_call x1, Pallas kernels, local(): pl.pallas_call(functools.partial(kernel, ep, tp), out_shape=jax.ShapeDtyp...  45.4 us
    unnamed x1, local copies, waits for them, and re-layouts  1.28 us

profile of v3, /device:TPU:1, one launch (start us, length us, event | category | flops | bytes accessed | tf_op | source)
XLA Modules:
  0.0 46.6 jit_solution(13432915713072688826)
XLA Ops:
  0.0 45.4 %layer.1 = bf16[16,128]{1,0:T(8,128)(2,1)} custom-call(bf16[16,2048]{1,0:T(8,128)(2,1)} %refs_0_.1, f32[1,2048]{1,0:T(1,128)} %bitcast.10, bf16[128,128]{1,0:T(8,128)(2,1)} %refs_2_.1, bf16[128,128]{1,0:T(8,128)(2,1)} %refs_3_.1, bf16[128,128]{1,0:T(8,128)(2,1)} %refs_4_.1, bf16[16,2048]{1,0:T(8,128)(2,1)} %bitcast.9, f32[1,16]{1,0:T(1,128)} %bitcast.14, ...), custom_call_target="tpu_custom_call" | custom-call | tf_op jit(solution)/shard_map/layer/pallas_call | solution.py:393
  45.4 1.3 %copy.22 = bf16[16,128]{1,0:T(8,128)(2,1)} copy(bf16[16,128]{1,0:T(8,128)(2,1)} %layer.1) | data formatting | bytes 8192

commit v4 on v3

v4 whole, which is shorter than its diff:
```python
import functools
import itertools

import jax
import jax.numpy as jnp
from jax import lax
from jax.experimental import pallas as pl
from jax.experimental.pallas import tpu as pltpu
from jax.sharding import PartitionSpec as P

MESH = pl.DeviceIdType.MESH
F32 = jnp.float32
BF16 = jnp.bfloat16
EPS = 1e-06
CAP = 2
LANES = 128

CH_X, CH_Q, CH_KV, CH_O, CH_R, CH_D, CH_DP, CH_RP = range(8)


def norm(v, gain):
    return v * lax.rsqrt(jnp.mean(v * v, axis=-1, keepdims=True) + EPS) * gain


def dot(a, b):
    return jnp.dot(a, b, preferred_element_type=F32)


def dot_t(a, b):
    return lax.dot_general(a, b, (((1,), (1,)), ((), ())), preferred_element_type=F32)


def hops(step, sizes):
    return sum(min(a, n - a) for a, n in zip(step, sizes))


def far_first(*sizes):
    steps = itertools.product(*(range(size) for size in sizes))
    return sorted(steps, key=lambda step: -hops(step, sizes))


def moved(me, size, step):
    return lax.rem(me + step, size) if step else me


def kernel(ep, tp, *refs):
    names = (
        "tokens", "norm_gain", "wq", "wk", "wv", "wf", "f_bias", "q_gain", "k_gain", "keys",
        "values", "gates", "lengths", "wo", "ffn_gain", "routes", "r_weights", "wg", "wu", "wd",
    )
    hbm = dict(zip(names, refs))
    out_ref = refs[len(names)]
    (
        tok_v, ng_v, wqkv_v, wf_v, fb_v, qg_v, kg_v, k_v, v_v, g_v, len_v,
        wo_v, fg_v, rt_v, rw_v, wgu_v, wd_v,
        xs, xr, qs, qr, kvs, kvr, os_, or_, ds_, dr, dp, rg, rp, rs, rr, kt, xe,
        hsem, ssem, rsem, dsem, dpsem, rpsem,
    ) = refs[len(names) + 1 :]

    me_e, me_t = lax.axis_index("ep"), lax.axis_index("tp")
    rows, width = tok_v.shape
    span, hd = k_v.shape[1], k_v.shape[2]
    depth = xs.shape[2]
    hidden = wd_v.shape[0] // 2
    slots = 2 * CAP
    n_slots = ep * slots

    outer, chips = ep // 4, tp // 2
    y, x = lax.div(me_e, 4), lax.rem(me_e, 4)
    z, core = lax.div(me_t, 2), lax.rem(me_t, 2)
    y_at = [moved(y, outer, a) for a in range(outer)]
    x_at = [moved(x, 4, a) for a in range(4)]
    z_at = [moved(z, chips, a) for a in range(chips)]
    core_at = [core, 1 - core]
    peers = {
        "ep": [y_at[a] * 4 + x_at[b] for a, b in far_first(outer, 4)[:-1]],
        "tp": [z_at[a] * 2 + core_at[b] for a, b in far_first(chips, 2)[:-1]],
    }
    partner = z * 2 + 1 - core
    chip_steps = [step for (step,) in far_first(chips)]
    chip_order = [z_at[step] for step in chip_steps]
    seen_as = {step: chip_steps.index(-step % chips) for step in chip_steps}
    barrier = pltpu.get_barrier_semaphore()
    for peer in peers["ep"]:
        pl.semaphore_signal(barrier, inc=1, device_id={"ep": peer}, device_id_type=MESH)
    for peer in peers["tp"]:
        pl.semaphore_signal(barrier, inc=1, device_id={"tp": peer}, device_id_type=MESH)

    fetches, taken = {}, itertools.count()

    def fetch(name, pairs, whole=None):
        waits, at = [], next(taken) if whole is not None else None
        for src, dst in pairs:
            sem = hsem.at[next(taken) if whole is None else at]
            copy = pltpu.make_async_copy(src, dst, sem)
            copy.start()
            waits.append(copy)
        fetches[name] = waits if whole is None else [pltpu.make_async_copy(whole, whole, sem)]

    def need(*which):
        for name in which:
            for copy in fetches[name]:
                copy.wait()

    fetch("tok", [(hbm["tokens"], tok_v), (hbm["norm_gain"], ng_v)])
    fetch(
        "wqkv",
        [(hbm[w], wqkv_v.at[:, pl.ds(i * hd, hd)]) for i, w in enumerate(("wq", "wk", "wv"))],
    )
    fetch(
        "small",
        [
            (hbm["wf"], wf_v), (hbm["f_bias"], fb_v), (hbm["q_gain"], qg_v),
            (hbm["k_gain"], kg_v), (hbm["gates"], g_v), (hbm["lengths"], len_v),
            (hbm["ffn_gain"], fg_v), (hbm["routes"], rt_v), (hbm["r_weights"], rw_v),
        ],
    )
    fetch("k", [(hbm["keys"].at[s, 0], k_v.at[s]) for s in range(rows)], k_v)

    def fetch_rest():
        fetch(
            "v",
            [
                (hbm["values"].at[s, 0], v_v.at[s // 2, :, pl.ds((s % 2) * hd, hd)])
                for s in range(rows)
            ],
            v_v,
        )
        fetch("wo", [(hbm["wo"], wo_v)])
        gated, downs = [], []
        for k, chip in enumerate(chip_order):
            for half, owner in enumerate((1 - core, core)):
                there = pl.ds(pl.multiple_of((2 * chip + owner) * LANES, LANES), LANES)
                here = pl.ds((half * chips + k) * LANES, LANES)
                after = pl.ds(((1 - half) * chips + k) * LANES, LANES)
                for i in range(2):
                    for n, w in enumerate(("wg", "wu")):
                        cols = pl.ds((2 * i + n) * hidden, hidden)
                        gated.append((hbm[w].at[i, there], wgu_v.at[here, cols]))
                    downs.append(
                        (hbm["wd"].at[i, :, there], wd_v.at[pl.ds(i * hidden, hidden), after])
                    )
        fetch("wgu", gated, wgu_v)
        fetch("wd", downs, wd_v)

    def send(axis, channel, to, src, dst):
        me = lax.axis_index(axis)
        for peer in to:
            pltpu.make_async_remote_copy(
                src_ref=src(peer),
                dst_ref=dst.at[me],
                send_sem=ssem.at[channel],
                recv_sem=rsem.at[channel],
                device_id={axis: peer},
                device_id_type=MESH,
            ).start()

    def wait_all(n, sem, buf):
        part = buf.at[pl.ds(0, n - 1)]
        pltpu.make_async_copy(part, part, sem).wait()

    need("tok")
    normed = norm(tok_v[...].astype(F32), ng_v[...]).astype(BF16)
    for j in range(ep):
        xs[j] = normed[:, j * depth : (j + 1) * depth]
    xr[pl.ds(me_e, 1)] = xs[pl.ds(me_e, 1)]
    pl.semaphore_wait(barrier, ep + tp - 2)
    send("ep", CH_X, peers["ep"], lambda j: xs.at[j], xr)
    fetch_rest()

    need("small")
    row = lax.broadcasted_iota(jnp.int32, (rows, 1), 0)
    diagonal = lax.broadcasted_iota(jnp.int32, (rows, rows), 0) == lax.broadcasted_iota(
        jnp.int32, (rows, rows), 1
    )

    def as_column(line):
        return jnp.sum(jnp.where(diagonal, line, jnp.zeros_like(line)), axis=1, keepdims=True)

    biased = dot_t(normed, wf_v[...]) + fb_v[...]
    own_head = lax.broadcasted_iota(jnp.int32, biased.shape, 1) == me_t
    biased = jnp.sum(jnp.where(own_head, biased, 0.0), axis=1, keepdims=True)
    forget = jnp.minimum(biased, 0.0) - jnp.log1p(jnp.exp(-jnp.abs(biased)))

    lengths = as_column(len_v[...].astype(F32)).astype(jnp.int32)
    position = lax.broadcasted_iota(jnp.int32, (rows, span), 1)
    gates = jnp.zeros((rows, span), F32)
    for s in range(rows):
        gates = jnp.where(row == s, g_v[s], gates)
    last_gate = jnp.sum(jnp.where(position == lengths - 1, gates, 0.0), axis=1, keepdims=True)
    bias = jnp.where(position < lengths, (last_gate - gates) + forget, -1e30)

    first = rt_v[0:1, :]
    second = rt_v[1:2, :]
    slot_col = lax.broadcasted_iota(jnp.int32, (n_slots, rows), 0)
    expert_col, copy_col = lax.div(slot_col, CAP), lax.rem(slot_col, CAP)
    named = ((expert_col == first) | (expert_col == second)).astype(F32)
    before = (
        lax.broadcasted_iota(jnp.int32, (rows, rows), 0)
        < lax.broadcasted_iota(jnp.int32, (rows, rows), 1)
    ).astype(F32)
    earlier = dot(named.astype(BF16), before.astype(BF16))
    placing = jnp.where(earlier == copy_col.astype(F32), named, 0.0).astype(BF16)

    weight_sum = rw_v[0:1, :] + rw_v[1:2, :]
    share_a = as_column(rw_v[0:1, :] / weight_sum)
    share_b = as_column(rw_v[1:2, :] / weight_sum)
    route_a = as_column(first.astype(F32)).astype(jnp.int32)
    route_b = as_column(second.astype(F32)).astype(jnp.int32)
    slot_row = lax.broadcasted_iota(jnp.int32, (rows, n_slots), 1)
    expert_row, copy_row = lax.div(slot_row, CAP), lax.rem(slot_row, CAP)
    is_a, is_b = expert_row == route_a, expert_row == route_b
    after = (
        lax.broadcasted_iota(jnp.int32, (rows, rows), 1)
        < lax.broadcasted_iota(jnp.int32, (rows, rows), 0)
    ).astype(BF16)
    earlier_row = dot(after, (is_a | is_b).astype(F32).astype(BF16))
    combine = jnp.where(is_a, share_a, 0.0) + jnp.where(is_b, share_b, 0.0)
    combine = jnp.where(earlier_row == copy_row.astype(F32), combine, 0.0)
    combine_1 = combine.astype(BF16)
    rest = combine - combine_1.astype(F32)
    combine_2 = rest.astype(BF16)
    combine_3 = (rest - combine_2.astype(F32)).astype(BF16)
    combine_parts = jnp.concatenate([combine_1, combine_2, combine_3], axis=0)

    need("k")
    for s in range(rows):
        kt[s * hd : (s + 1) * hd, :] = k_v[s].T

    need("wqkv")
    wait_all(ep, rsem.at[CH_X], xr)
    part = dot(xr[...].reshape(ep * rows, depth), wqkv_v[...])
    qs[...] = part[:, :hd].reshape(ep, rows, hd)
    send("ep", CH_Q, peers["ep"], lambda j: qs.at[j], qr)
    for j in range(ep):
        own = part[j * rows : (j + 1) * rows]
        kvs[j, 0:rows, :] = own[:, hd : 2 * hd].astype(BF16)
        kvs[j, rows : 2 * rows, :] = own[:, 2 * hd :].astype(BF16)
    send("ep", CH_KV, peers["ep"], lambda j: kvs.at[j], kvr)
    qr[pl.ds(me_e, 1)] = qs[pl.ds(me_e, 1)]
    kvr[pl.ds(me_e, 1)] = kvs[pl.ds(me_e, 1)]
    need("v")
    wait_all(ep, rsem.at[CH_Q], qr)
    queries = norm(jnp.sum(qr[...], axis=0), qg_v[...]).astype(BF16)

    score_scale = hd ** (-0.5)
    wide = queries.astype(F32)
    scores = jnp.zeros((rows, span), F32)
    for pair in range(rows // 2):
        both = [jnp.where(row == 2 * pair + i, wide, 0.0) for i in range(2)]
        both = jnp.concatenate(both, axis=1).astype(BF16)
        scores = scores + dot(both, kt[2 * pair * hd : (2 * pair + 2) * hd, :])
    wait_all(ep, rsem.at[CH_KV], kvr)
    kv_raw = jnp.sum(kvr[...].astype(F32), axis=0)
    keys_new = norm(kv_raw[:rows], kg_v[...]).astype(BF16)
    values_new = kv_raw[rows:].astype(BF16)
    scores = scores * score_scale + bias
    own_score = (
        jnp.sum(queries.astype(F32) * keys_new.astype(F32), axis=1, keepdims=True) * score_scale
    )
    peak = jnp.maximum(jnp.max(scores, axis=1, keepdims=True), own_score)
    weights = jnp.exp(scores - peak)
    own_weight = jnp.exp(own_score - peak)
    denominator = jnp.sum(weights, axis=1, keepdims=True) + own_weight
    probabilities = weights / denominator
    own_prob = (own_weight / denominator).astype(BF16).astype(F32)
    apart = [
        jnp.where(lax.div(row, 2) == pair, probabilities, 0.0).astype(BF16)
        for pair in range(rows // 2)
    ]
    summed = dot(jnp.concatenate(apart, axis=1), v_v[...].reshape(rows // 2 * span, 2 * hd))
    summed = jnp.where(lax.rem(row, 2) == 0, summed[:, :hd], summed[:, hd:])
    attended = (summed + own_prob * values_new.astype(F32)).astype(BF16)

    need("wo")
    cols = or_.shape[2]
    partial = dot(attended, wo_v[...])
    for j in range(tp):
        os_[j] = partial[:, j * cols : (j + 1) * cols].astype(BF16)
    or_[pl.ds(me_t, 1)] = os_[pl.ds(me_t, 1)]
    send("tp", CH_O, peers["tp"], lambda j: os_.at[j], or_)
    wait_all(tp, rsem.at[CH_O], or_)
    own_tokens = tok_v[:, pl.ds(pl.multiple_of(me_t * cols, cols), cols)].astype(F32)
    mixed = (own_tokens + jnp.sum(or_[...].astype(F32), axis=0)).astype(BF16)

    def send_rows(channel, src, dst, recv_sem, step):
        a, b, d = step
        owner = y_at[a] * 4 + x_at[b]
        k = seen_as[d]
        pltpu.make_async_remote_copy(
            src_ref=src(slots * owner),
            dst_ref=dst.at[pl.ds(k * n_slots + slots * me_e, slots)],
            send_sem=ssem.at[channel],
            recv_sem=recv_sem(k),
            device_id={"ep": owner, "tp": z_at[d] * 2 + 1 - core},
            device_id_type=MESH,
        ).start()

    def swap(channel, src, dst, sem, at):
        pltpu.make_async_remote_copy(
            src_ref=src.at[at],
            dst_ref=dst.at[at],
            send_sem=ssem.at[channel],
            recv_sem=sem,
            device_id={"tp": partner},
            device_id_type=MESH,
        ).start()

    def wait_rows(sem, buf):
        pltpu.make_async_copy(buf, buf, sem).wait()

    def block_rows(k, count=1):
        return pl.ds(k * n_slots, count * n_slots)

    ds_[...] = dot(placing, mixed).astype(BF16)
    for step in far_first(outer, 4, chips):
        send_rows(CH_D, lambda at: ds_.at[pl.ds(at, slots)], dr, lambda k: dsem.at[k], step)
    need("wgu", "wd")
    squares = jnp.zeros((n_slots, LANES), F32)
    for k in reversed(range(chips)):
        wait_rows(dsem.at[k], dr.at[block_rows(k)])
        swap(CH_DP, dr, dp, dpsem.at[k], block_rows(k))
        block = dr[block_rows(k), :].astype(F32)
        squares = squares + block * block
    for k in reversed(range(chips)):
        wait_rows(dpsem.at[k], dp.at[block_rows(k)])
        block = dp[block_rows(k), :].astype(F32)
        squares = squares + block * block
    factor = lax.rsqrt(jnp.sum(squares, axis=1, keepdims=True) / width + EPS)
    for half, (buf, owner) in enumerate(((dr, 1 - core), (dp, core))):
        for k, chip in enumerate(chip_order):
            at = pl.multiple_of((2 * chip + owner) * LANES, LANES)
            block = buf[block_rows(k), :].astype(F32) * factor * fg_v[:, pl.ds(at, LANES)]
            here = (half * chips + k) * LANES
            xe[:, here : here + LANES] = block.astype(BF16)

    both = dot(xe[...], wgu_v[...])
    slot_line = lax.broadcasted_iota(jnp.int32, (n_slots, 1), 0)
    kind = lax.div(lax.rem(slot_line, slots), CAP)
    parts = []
    for i in range(2):
        gate = both[:, 2 * i * hidden : (2 * i + 1) * hidden]
        upper = both[:, (2 * i + 1) * hidden : (2 * i + 2) * hidden]
        parts.append(jnp.where(kind == i, gate * jax.nn.sigmoid(gate) * upper, 0.0))
    hidden_rows = jnp.concatenate(parts, axis=1).astype(BF16)

    halves = min(2, chips)
    share = chips // halves
    for half in range(halves):
        first_col = half * share * LANES
        given = dot(hidden_rows, wd_v[:, first_col : first_col + share * LANES]).astype(BF16)
        for n in range(share):
            rg[block_rows(half * share + n), :] = given[:, n * LANES : (n + 1) * LANES]
        swap(CH_RP, rg, rp, rpsem.at[half], block_rows(half * share, share))
    kept = dot(hidden_rows, wd_v[:, chips * LANES :])
    for half in range(halves):
        wait_rows(rpsem.at[half], rp.at[block_rows(half * share, share)])
        for k in range(half * share, (half + 1) * share):
            mine = kept[:, k * LANES : (k + 1) * LANES]
            rs[block_rows(k), :] = (mine + rp[block_rows(k), :].astype(F32)).astype(BF16)
        for a, b, d in far_first(outer, 4, chips):
            k = chip_steps.index(d)
            if k // share == half:
                send_rows(
                    CH_R,
                    lambda at: rs.at[pl.ds(k * n_slots + at, slots)],
                    rr,
                    lambda _: rsem.at[CH_R],
                    (a, b, d),
                )
    wait_rows(rsem.at[CH_R], rr)

    total = jnp.zeros((n_slots, LANES), F32)
    for k in range(chips):
        total = total + rr[block_rows(k), :].astype(F32)
    stacked = dot(combine_parts, total.astype(BF16))
    mix = stacked[:rows] + stacked[rows : 2 * rows] + stacked[2 * rows :]
    out_ref[...] = (mixed.astype(F32) + mix).astype(BF16)

    for channel, n, buf in ((CH_X, ep, xs), (CH_Q, ep, qs), (CH_KV, ep, kvs), (CH_O, tp, os_)):
        wait_all(n, ssem.at[channel], buf)
    for channel, buf in ((CH_D, dr), (CH_DP, dr), (CH_RP, rg), (CH_R, rs)):
        wait_rows(ssem.at[channel], buf)


def local(ep, tp, tokens, norm_gain, w_query, w_key, w_value, w_forget, forget_bias, query_gain,
          key_gain, cache_keys, cache_values, cache_gates, lengths, w_output, ffn_gain, routes,
          route_weights, w_gate, w_up, w_down):
    rows, width = tokens.shape
    span, hd = cache_keys.shape[2], cache_keys.shape[3]
    depth = w_query.shape[0]
    cols = width // tp
    hidden = w_gate.shape[2]
    heads = w_forget.shape[1]
    n_slots = 2 * CAP * ep
    vmem = pltpu.VMEM
    scratch = [
        vmem((rows, width), BF16), vmem((1, width), F32), vmem((depth, 3 * hd), BF16),
        vmem((heads, width), BF16), vmem((1, heads), F32), vmem((1, hd), F32), vmem((1, hd), F32),
        vmem((rows, span, hd), BF16), vmem((rows // 2, span, 2 * hd), BF16), vmem((rows, 1, span), F32),
        vmem((1, rows), jnp.int32), vmem((hd, width), BF16), vmem((1, width), F32),
        vmem((2, rows), jnp.int32), vmem((2, rows), F32), vmem((width, 4 * hidden), BF16),
        vmem((2 * hidden, width), BF16),
        vmem((ep, rows, depth), BF16), vmem((ep, rows, depth), BF16),
        vmem((ep, rows, hd), F32), vmem((ep, rows, hd), F32),
        vmem((ep, 2 * rows, hd), BF16), vmem((ep, 2 * rows, hd), BF16),
        vmem((tp, rows, cols), BF16), vmem((tp, rows, cols), BF16),
        vmem((n_slots, LANES), BF16), *[vmem((tp // 2 * n_slots, LANES), BF16)] * 6,
        vmem((rows * hd, span), BF16), vmem((n_slots, width), BF16),
        pltpu.SemaphoreType.DMA((24,)), pltpu.SemaphoreType.DMA((8,)),
        pltpu.SemaphoreType.DMA((5,)), *[pltpu.SemaphoreType.DMA((tp // 2,))] * 3,
    ]
    operands = (
        tokens, norm_gain[None], w_query, w_key, w_value, w_forget.T, forget_bias[None],
        query_gain[None], key_gain[None], cache_keys, cache_values, cache_gates, lengths[None],
        w_output, ffn_gain[None], routes.T, route_weights.T, w_gate, w_up, w_down,
    )
    return pl.pallas_call(
        functools.partial(kernel, ep, tp),
        out_shape=pltpu.VMEM((rows, cols), BF16),
        in_specs=[pl.BlockSpec(memory_space=pltpu.HBM)] * len(operands),
        out_specs=pl.BlockSpec(memory_space=pltpu.VMEM),
        scratch_shapes=scratch,
        compiler_params=pltpu.CompilerParams(
            collective_id=0, has_side_effects=True, vmem_limit_bytes=67043328 - 65536
        ),
        name="layer",
    )(*operands)


def solution(mesh):
    placed = (
        P("ep", None), P(), P("ep", "tp"), P("ep", "tp"), P("ep", "tp"), P(), P(), P(), P(),
        P("ep", "tp", None, None), P("ep", "tp", None, None), P("ep", "tp", None), P("ep"),
        P("tp", None), P(), P("ep", None), P("ep", None), P("ep", None, "tp"),
        P("ep", None, "tp"), P("ep", "tp", None),
    )
    return jax.shard_map(
        functools.partial(local, mesh.shape["ep"], mesh.shape["tp"]),
        mesh=mesh, in_specs=placed, out_specs=P("ep", "tp"), check_vma=False,
    )
```

time: 46.8 us -> 45.6 us (0.974)
  local copies, waits for them, and re-layouts: 1.28 us -> 0.6 us
    unnamed x1, local copies, waits for them, and re-layouts: 1.28 us -> 0.6 us
where the time goes in v4:
time: 45.6 us
  Pallas kernels  45 us (99%)
  local copies, waits for them, and re-layouts  0.6 us (1%)
    pallas_call x1, Pallas kernels, local(): pl.pallas_call(functools.partial(kernel, ep, tp), out_shape=pltpu.VMEM((r...  45 us

profile of v4, /device:TPU:1, one launch (start us, length us, event | category | flops | bytes accessed | tf_op | source)
XLA Modules:
  0.0 45.6 jit_solution(5086416242722366898)
XLA Ops:
  0.0 45.0 %layer.1 = bf16[16,128]{1,0:T(8,128)(2,1)S(1)} custom-call(bf16[16,2048]{1,0:T(8,128)(2,1)} %refs_0_.1, f32[1,2048]{1,0:T(1,128)} %bitcast.10, bf16[128,128]{1,0:T(8,128)(2,1)} %refs_2_.1, bf16[128,128]{1,0:T(8,128)(2,1)} %refs_3_.1, bf16[128,128]{1,0:T(8,128)(2,1)} %refs_4_.1, bf16[16,2048]{1,0:T(8,128)(2,1)} %bitcast.9, f32[1,16]{1,0:T(1,128)} %bitcast.14, ...), custom_call_target="tpu_custom_call" | custom-call | tf_op jit(solution)/shard_map/layer/pallas_call | solution.py:418
  45.0 0.6 %copy.22 = bf16[16,128]{1,0:T(8,128)(2,1)} copy(bf16[16,128]{1,0:T(8,128)(2,1)S(1)} %layer.1) | data formatting | bytes 8192

commit v5 on v4

--- a/solution.py
+++ b/solution.py
@@ -15,7 +15,8 @@
 CAP = 2
 LANES = 128
 
-CH_X, CH_Q, CH_KV, CH_O, CH_R, CH_D, CH_DP, CH_RP = range(8)
+CH_X, CH_Q, CH_KV, CH_O, CH_R, CH_WQ, CH_WKV, CH_D, CH_DP, CH_RP = range(10)
+SHARERS = 8
 
 
 def norm(v, gain):
@@ -51,7 +52,7 @@
     hbm = dict(zip(names, refs))
     out_ref = refs[len(names)]
     (
-        tok_v, ng_v, wqkv_v, wf_v, fb_v, qg_v, kg_v, k_v, v_v, g_v, len_v,
+        tok_v, ng_v, wq_v, wkv_v, wf_v, fb_v, qg_v, kg_v, k_v, v_v, g_v, len_v,
         wo_v, fg_v, rt_v, rw_v, wgu_v, wd_v,
         xs, xr, qs, qr, kvs, kvr, os_, or_, ds_, dr, dp, rg, rp, rs, rr, kt, xe,
         hsem, ssem, rsem, dsem, dpsem, rpsem,
@@ -64,27 +65,6 @@
     hidden = wd_v.shape[0] // 2
     slots = 2 * CAP
     n_slots = ep * slots
-
-    outer, chips = ep // 4, tp // 2
-    y, x = lax.div(me_e, 4), lax.rem(me_e, 4)
-    z, core = lax.div(me_t, 2), lax.rem(me_t, 2)
-    y_at = [moved(y, outer, a) for a in range(outer)]
-    x_at = [moved(x, 4, a) for a in range(4)]
-    z_at = [moved(z, chips, a) for a in range(chips)]
-    core_at = [core, 1 - core]
-    peers = {
-        "ep": [y_at[a] * 4 + x_at[b] for a, b in far_first(outer, 4)[:-1]],
-        "tp": [z_at[a] * 2 + core_at[b] for a, b in far_first(chips, 2)[:-1]],
-    }
-    partner = z * 2 + 1 - core
-    chip_steps = [step for (step,) in far_first(chips)]
-    chip_order = [z_at[step] for step in chip_steps]
-    seen_as = {step: chip_steps.index(-step % chips) for step in chip_steps}
-    barrier = pltpu.get_barrier_semaphore()
-    for peer in peers["ep"]:
-        pl.semaphore_signal(barrier, inc=1, device_id={"ep": peer}, device_id_type=MESH)
-    for peer in peers["tp"]:
-        pl.semaphore_signal(barrier, inc=1, device_id={"tp": peer}, device_id_type=MESH)
 
     fetches, taken = {}, itertools.count()
 
@@ -103,9 +83,36 @@
                 copy.wait()
 
     fetch("tok", [(hbm["tokens"], tok_v), (hbm["norm_gain"], ng_v)])
+
+    outer, chips = ep // 4, tp // 2
+    y, x = lax.div(me_e, 4), lax.rem(me_e, 4)
+    z, core = lax.div(me_t, 2), lax.rem(me_t, 2)
+    y_at = [moved(y, outer, a) for a in range(outer)]
+    x_at = [moved(x, 4, a) for a in range(4)]
+    z_at = [moved(z, chips, a) for a in range(chips)]
+    core_at = [core, 1 - core]
+    turn = 2 * lax.rem(y, 2)
+    y_weights, y_tokens = y + 1 - turn, lax.rem(y + outer - 1 + turn, outer)
+    sharers = [(a, x_at[b]) for a, b in far_first(2, 4)[:-1]]
+    y_of = (y, y_tokens)
+    others = [z_at[a] * 2 + core_at[b] for a, b in far_first(chips, 2)[:-1]]
+    partner = z * 2 + 1 - core
+    chip_steps = [step for (step,) in far_first(chips)]
+    chip_order = [z_at[step] for step in chip_steps]
+    seen_as = {step: chip_steps.index(-step % chips) for step in chip_steps}
+    barrier = pltpu.get_barrier_semaphore()
+    for peer in [y_of[a] * 4 + b for a, b in sharers] + [y_weights * 4 + x]:
+        pl.semaphore_signal(barrier, inc=1, device_id={"ep": peer}, device_id_type=MESH)
+    for peer in others:
+        pl.semaphore_signal(barrier, inc=1, device_id={"tp": peer}, device_id_type=MESH)
+
     fetch(
         "wqkv",
-        [(hbm[w], wqkv_v.at[:, pl.ds(i * hd, hd)]) for i, w in enumerate(("wq", "wk", "wv"))],
+        [
+            (hbm["wq"], wq_v.at[pl.ds(0, depth)]),
+            (hbm["wk"], wkv_v.at[pl.ds(0, depth), pl.ds(0, hd)]),
+            (hbm["wv"], wkv_v.at[pl.ds(0, depth), pl.ds(hd, hd)]),
+        ],
     )
     fetch(
         "small",
@@ -143,17 +150,18 @@
         fetch("wgu", gated, wgu_v)
         fetch("wd", downs, wd_v)
 
-    def send(axis, channel, to, src, dst):
-        me = lax.axis_index(axis)
-        for peer in to:
-            pltpu.make_async_remote_copy(
-                src_ref=src(peer),
-                dst_ref=dst.at[me],
-                send_sem=ssem.at[channel],
-                recv_sem=rsem.at[channel],
-                device_id={axis: peer},
-                device_id_type=MESH,
-            ).start()
+    def send(channel, src, dst, **to):
+        pltpu.make_async_remote_copy(
+            src_ref=src,
+            dst_ref=dst,
+            send_sem=ssem.at[channel],
+            recv_sem=rsem.at[channel],
+            device_id=to,
+            device_id_type=MESH,
+        ).start()
+
+    def wait_copy(sem, buf):
+        pltpu.make_async_copy(buf, buf, sem).wait()
 
     def wait_all(n, sem, buf):
         part = buf.at[pl.ds(0, n - 1)]
@@ -163,9 +171,18 @@
     normed = norm(tok_v[...].astype(F32), ng_v[...]).astype(BF16)
     for j in range(ep):
         xs[j] = normed[:, j * depth : (j + 1) * depth]
-    xr[pl.ds(me_e, 1)] = xs[pl.ds(me_e, 1)]
-    pl.semaphore_wait(barrier, ep + tp - 2)
-    send("ep", CH_X, peers["ep"], lambda j: xs.at[j], xr)
+    xr[pl.ds(x, 1)] = xs[pl.ds(me_e, 1)]
+    xr[pl.ds(SHARERS + x, 1)] = xs[pl.ds(y_weights * 4 + x, 1)]
+    need("wqkv")
+    pl.semaphore_wait(barrier, SHARERS + tp - 1)
+    own_rows, new_rows = pl.ds(0, depth), pl.ds(depth, depth)
+    send(CH_WQ, wq_v.at[own_rows], wq_v.at[new_rows], ep=y_weights * 4 + x)
+    blocks_of = ((y, y_weights), (y_tokens, y_tokens + 1 - 2 * lax.rem(y_tokens, 2)))
+    for a, b in sharers:
+        for n, y_block in enumerate(blocks_of[a]):
+            there = xr.at[n * SHARERS + 4 * a + x]
+            send(CH_X, xs.at[y_block * 4 + b], there, ep=y_of[a] * 4 + b)
+    send(CH_WKV, wkv_v.at[own_rows], wkv_v.at[new_rows], ep=y_weights * 4 + x)
     fetch_rest()
 
     need("small")
@@ -223,24 +240,33 @@
     combine_3 = (rest - combine_2.astype(F32)).astype(BF16)
     combine_parts = jnp.concatenate([combine_1, combine_2, combine_3], axis=0)
 
+    def turn_keys(first_row, last_row):
+        for s in range(first_row, last_row):
+            kt[s * hd : (s + 1) * hd, :] = k_v[s].T
+
     need("k")
-    for s in range(rows):
-        kt[s * hd : (s + 1) * hd, :] = k_v[s].T
-
-    need("wqkv")
-    wait_all(ep, rsem.at[CH_X], xr)
-    part = dot(xr[...].reshape(ep * rows, depth), wqkv_v[...])
-    qs[...] = part[:, :hd].reshape(ep, rows, hd)
-    send("ep", CH_Q, peers["ep"], lambda j: qs.at[j], qr)
-    for j in range(ep):
+    turn_keys(0, rows // 2)
+
+    wait_copy(rsem.at[CH_WQ], wq_v.at[new_rows])
+    wait_copy(rsem.at[CH_X], xr.at[pl.ds(0, 2 * (SHARERS - 1))])
+    inputs = xr[...].reshape(2, SHARERS * rows, depth)
+    inputs = jnp.concatenate([inputs[0], inputs[1]], axis=1)
+    qs[...] = dot(inputs, wq_v[...]).reshape(SHARERS, rows, hd)
+    for a, b in sharers:
+        send(CH_Q, qs.at[4 * a + b], qr.at[4 * a + x], ep=y_of[a] * 4 + b)
+    turn_keys(rows // 2, rows)
+    wait_copy(rsem.at[CH_WKV], wkv_v.at[new_rows])
+    part = dot(inputs, wkv_v[...])
+    for j in range(SHARERS):
         own = part[j * rows : (j + 1) * rows]
-        kvs[j, 0:rows, :] = own[:, hd : 2 * hd].astype(BF16)
-        kvs[j, rows : 2 * rows, :] = own[:, 2 * hd :].astype(BF16)
-    send("ep", CH_KV, peers["ep"], lambda j: kvs.at[j], kvr)
-    qr[pl.ds(me_e, 1)] = qs[pl.ds(me_e, 1)]
-    kvr[pl.ds(me_e, 1)] = kvs[pl.ds(me_e, 1)]
+        kvs[j, 0:rows, :] = own[:, :hd].astype(BF16)
+        kvs[j, rows : 2 * rows, :] = own[:, hd:].astype(BF16)
+    for a, b in sharers:
+        send(CH_KV, kvs.at[4 * a + b], kvr.at[4 * a + x], ep=y_of[a] * 4 + b)
+    qr[pl.ds(x, 1)] = qs[pl.ds(x, 1)]
+    kvr[pl.ds(x, 1)] = kvs[pl.ds(x, 1)]
     need("v")
-    wait_all(ep, rsem.at[CH_Q], qr)
+    wait_all(SHARERS, rsem.at[CH_Q], qr)
     queries = norm(jnp.sum(qr[...], axis=0), qg_v[...]).astype(BF16)
 
     score_scale = hd ** (-0.5)
@@ -250,7 +276,7 @@
         both = [jnp.where(row == 2 * pair + i, wide, 0.0) for i in range(2)]
         both = jnp.concatenate(both, axis=1).astype(BF16)
         scores = scores + dot(both, kt[2 * pair * hd : (2 * pair + 2) * hd, :])
-    wait_all(ep, rsem.at[CH_KV], kvr)
+    wait_all(SHARERS, rsem.at[CH_KV], kvr)
     kv_raw = jnp.sum(kvr[...].astype(F32), axis=0)
     keys_new = norm(kv_raw[:rows], kg_v[...]).astype(BF16)
     values_new = kv_raw[rows:].astype(BF16)
@@ -258,11 +284,13 @@
     own_score = (
         jnp.sum(queries.astype(F32) * keys_new.astype(F32), axis=1, keepdims=True) * score_scale
     )
-    peak = jnp.maximum(jnp.max(scores, axis=1, keepdims=True), own_score)
-    weights = jnp.exp(scores - peak)
+    cached_peak = jnp.max(scores, axis=1, keepdims=True)
+    weights = jnp.exp(scores - cached_peak)
+    peak = jnp.maximum(cached_peak, own_score)
+    lowered = jnp.exp(cached_peak - peak)
     own_weight = jnp.exp(own_score - peak)
-    denominator = jnp.sum(weights, axis=1, keepdims=True) + own_weight
-    probabilities = weights / denominator
+    denominator = jnp.sum(weights, axis=1, keepdims=True) * lowered + own_weight
+    probabilities = weights * (lowered / denominator)
     own_prob = (own_weight / denominator).astype(BF16).astype(F32)
     apart = [
         jnp.where(lax.div(row, 2) == pair, probabilities, 0.0).astype(BF16)
@@ -278,7 +306,8 @@
     for j in range(tp):
         os_[j] = partial[:, j * cols : (j + 1) * cols].astype(BF16)
     or_[pl.ds(me_t, 1)] = os_[pl.ds(me_t, 1)]
-    send("tp", CH_O, peers["tp"], lambda j: os_.at[j], or_)
+    for peer in others:
+        send(CH_O, os_.at[peer], or_.at[me_t], tp=peer)
     wait_all(tp, rsem.at[CH_O], or_)
     own_tokens = tok_v[:, pl.ds(pl.multiple_of(me_t * cols, cols), cols)].astype(F32)
     mixed = (own_tokens + jnp.sum(or_[...].astype(F32), axis=0)).astype(BF16)
@@ -306,9 +335,6 @@
             device_id_type=MESH,
         ).start()
 
-    def wait_rows(sem, buf):
-        pltpu.make_async_copy(buf, buf, sem).wait()
-
     def block_rows(k, count=1):
         return pl.ds(k * n_slots, count * n_slots)
 
@@ -318,12 +344,12 @@
     need("wgu", "wd")
     squares = jnp.zeros((n_slots, LANES), F32)
     for k in reversed(range(chips)):
-        wait_rows(dsem.at[k], dr.at[block_rows(k)])
+        wait_copy(dsem.at[k], dr.at[block_rows(k)])
         swap(CH_DP, dr, dp, dpsem.at[k], block_rows(k))
         block = dr[block_rows(k), :].astype(F32)
         squares = squares + block * block
     for k in reversed(range(chips)):
-        wait_rows(dpsem.at[k], dp.at[block_rows(k)])
+        wait_copy(dpsem.at[k], dp.at[block_rows(k)])
         block = dp[block_rows(k), :].astype(F32)
         squares = squares + block * block
     factor = lax.rsqrt(jnp.sum(squares, axis=1, keepdims=True) / width + EPS)
@@ -354,7 +380,7 @@
         swap(CH_RP, rg, rp, rpsem.at[half], block_rows(half * share, share))
     kept = dot(hidden_rows, wd_v[:, chips * LANES :])
     for half in range(halves):
-        wait_rows(rpsem.at[half], rp.at[block_rows(half * share, share)])
+        wait_copy(rpsem.at[half], rp.at[block_rows(half * share, share)])
         for k in range(half * share, (half + 1) * share):
             mine = kept[:, k * LANES : (k + 1) * LANES]
             rs[block_rows(k), :] = (mine + rp[block_rows(k), :].astype(F32)).astype(BF16)
@@ -368,7 +394,7 @@
                     lambda _: rsem.at[CH_R],
                     (a, b, d),
                 )
-    wait_rows(rsem.at[CH_R], rr)
+    wait_copy(rsem.at[CH_R], rr)
 
     total = jnp.zeros((n_slots, LANES), F32)
     for k in range(chips):
@@ -377,10 +403,13 @@
     mix = stacked[:rows] + stacked[rows : 2 * rows] + stacked[2 * rows :]
     out_ref[...] = (mixed.astype(F32) + mix).astype(BF16)
 
-    for channel, n, buf in ((CH_X, ep, xs), (CH_Q, ep, qs), (CH_KV, ep, kvs), (CH_O, tp, os_)):
+    for channel, n, buf in ((CH_Q, SHARERS, qs), (CH_KV, SHARERS, kvs), (CH_O, tp, os_)):
         wait_all(n, ssem.at[channel], buf)
+    wait_copy(ssem.at[CH_X], xr.at[pl.ds(0, 2 * (SHARERS - 1))])
+    wait_copy(ssem.at[CH_WQ], wq_v.at[own_rows])
+    wait_copy(ssem.at[CH_WKV], wkv_v.at[own_rows])
     for channel, buf in ((CH_D, dr), (CH_DP, dr), (CH_RP, rg), (CH_R, rs)):
-        wait_rows(ssem.at[channel], buf)
+        wait_copy(ssem.at[channel], buf)
 
 
 def local(ep, tp, tokens, norm_gain, w_query, w_key, w_value, w_forget, forget_bias, query_gain,
@@ -395,20 +424,21 @@
     n_slots = 2 * CAP * ep
     vmem = pltpu.VMEM
     scratch = [
-        vmem((rows, width), BF16), vmem((1, width), F32), vmem((depth, 3 * hd), BF16),
+        vmem((rows, width), BF16), vmem((1, width), F32), vmem((2 * depth, hd), BF16),
+        vmem((2 * depth, 2 * hd), BF16),
         vmem((heads, width), BF16), vmem((1, heads), F32), vmem((1, hd), F32), vmem((1, hd), F32),
         vmem((rows, span, hd), BF16), vmem((rows // 2, span, 2 * hd), BF16), vmem((rows, 1, span), F32),
         vmem((1, rows), jnp.int32), vmem((hd, width), BF16), vmem((1, width), F32),
         vmem((2, rows), jnp.int32), vmem((2, rows), F32), vmem((width, 4 * hidden), BF16),
         vmem((2 * hidden, width), BF16),
-        vmem((ep, rows, depth), BF16), vmem((ep, rows, depth), BF16),
-        vmem((ep, rows, hd), F32), vmem((ep, rows, hd), F32),
-        vmem((ep, 2 * rows, hd), BF16), vmem((ep, 2 * rows, hd), BF16),
+        vmem((ep, rows, depth), BF16), vmem((2 * SHARERS, rows, depth), BF16),
+        vmem((SHARERS, rows, hd), F32), vmem((SHARERS, rows, hd), F32),
+        vmem((SHARERS, 2 * rows, hd), BF16), vmem((SHARERS, 2 * rows, hd), BF16),
         vmem((tp, rows, cols), BF16), vmem((tp, rows, cols), BF16),
         vmem((n_slots, LANES), BF16), *[vmem((tp // 2 * n_slots, LANES), BF16)] * 6,
         vmem((rows * hd, span), BF16), vmem((n_slots, width), BF16),
-        pltpu.SemaphoreType.DMA((24,)), pltpu.SemaphoreType.DMA((8,)),
-        pltpu.SemaphoreType.DMA((5,)), *[pltpu.SemaphoreType.DMA((tp // 2,))] * 3,
+        pltpu.SemaphoreType.DMA((24,)), pltpu.SemaphoreType.DMA((10,)),
+        pltpu.SemaphoreType.DMA((7,)), *[pltpu.SemaphoreType.DMA((tp // 2,))] * 3,
     ]
     operands = (
         tokens, norm_gain[None], w_query, w_key, w_value, w_forget.T, forget_bias[None],

time: 45.6 us -> 45.4 us (level)
  no operation moved by 1% of the time
where the time goes in v5:
time: 45.4 us
  Pallas kernels  44.7 us (98%)
  local copies, waits for them, and re-layouts  0.6 us (1%)
    pallas_call x1, Pallas kernels, local(): pl.pallas_call(functools.partial(kernel, ep, tp), out_shape=pltpu.VMEM((r...  44.7 us

profile of v5, /device:TPU:1, one launch (start us, length us, event | category | flops | bytes accessed | tf_op | source)
XLA Modules:
  0.0 45.4 jit_solution(13845527312316740979)
XLA Ops:
  0.0 44.7 %layer.1 = bf16[16,128]{1,0:T(8,128)(2,1)S(1)} custom-call(bf16[16,2048]{1,0:T(8,128)(2,1)} %refs_0_.1, f32[1,2048]{1,0:T(1,128)} %bitcast.10, bf16[128,128]{1,0:T(8,128)(2,1)} %refs_2_.1, bf16[128,128]{1,0:T(8,128)(2,1)} %refs_3_.1, bf16[128,128]{1,0:T(8,128)(2,1)} %refs_4_.1, bf16[16,2048]{1,0:T(8,128)(2,1)} %bitcast.9, f32[1,16]{1,0:T(1,128)} %bitcast.14, ...), custom_call_target="tpu_custom_call" | custom-call | tf_op jit(solution)/shard_map/layer/pallas_call | solution.py:448
  44.8 0.6 %copy.22 = bf16[16,128]{1,0:T(8,128)(2,1)} copy(bf16[16,128]{1,0:T(8,128)(2,1)S(1)} %layer.1) | data formatting | bytes 8192

commit v6 on v5

--- a/solution.py
+++ b/solution.py
@@ -290,14 +290,13 @@
     lowered = jnp.exp(cached_peak - peak)
     own_weight = jnp.exp(own_score - peak)
     denominator = jnp.sum(weights, axis=1, keepdims=True) * lowered + own_weight
-    probabilities = weights * (lowered / denominator)
     own_prob = (own_weight / denominator).astype(BF16).astype(F32)
     apart = [
-        jnp.where(lax.div(row, 2) == pair, probabilities, 0.0).astype(BF16)
-        for pair in range(rows // 2)
+        jnp.where(lax.div(row, 2) == pair, weights, 0.0).astype(BF16) for pair in range(rows // 2)
     ]
     summed = dot(jnp.concatenate(apart, axis=1), v_v[...].reshape(rows // 2 * span, 2 * hd))
     summed = jnp.where(lax.rem(row, 2) == 0, summed[:, :hd], summed[:, hd:])
+    summed = summed * (lowered / denominator)
     attended = (summed + own_prob * values_new.astype(F32)).astype(BF16)
 
     need("wo")

time: 45.4 us -> 45.3 us (level)
  no operation moved by 1% of the time
where the time goes in v6:
time: 45.3 us; the launch traced here: 45.2 us
  Pallas kernels  44.6 us (98%)
  local copies, waits for them, and re-layouts  0.6 us (1%)
    pallas_call x1, Pallas kernels, local(): pl.pallas_call(functools.partial(kernel, ep, tp), out_shape=pltpu.VMEM((r...  44.6 us

profile of v6, /device:TPU:1, one launch (start us, length us, event | category | flops | bytes accessed | tf_op | source)
XLA Modules:
  0.0 45.2 jit_solution(10933563319942233162)
XLA Ops:
  0.0 44.6 %layer.1 = bf16[16,128]{1,0:T(8,128)(2,1)S(1)} custom-call(bf16[16,2048]{1,0:T(8,128)(2,1)} %refs_0_.1, f32[1,2048]{1,0:T(1,128)} %bitcast.10, bf16[128,128]{1,0:T(8,128)(2,1)} %refs_2_.1, bf16[128,128]{1,0:T(8,128)(2,1)} %refs_3_.1, bf16[128,128]{1,0:T(8,128)(2,1)} %refs_4_.1, bf16[16,2048]{1,0:T(8,128)(2,1)} %bitcast.9, f32[1,16]{1,0:T(1,128)} %bitcast.14, ...), custom_call_target="tpu_custom_call" | custom-call | tf_op jit(solution)/shard_map/layer/pallas_call | solution.py:447
  44.7 0.6 %copy.22 = bf16[16,128]{1,0:T(8,128)(2,1)} copy(bf16[16,128]{1,0:T(8,128)(2,1)S(1)} %layer.1) | data formatting | bytes 8192
